TPU v7x, 32 devices: a whole 2x2x4 slice. The times are simulated.
32 devices in a mesh: grp: 2 (over y), kv: 4 (over z), tp: 4 (over x, core).
Axes of the slice: x: 2, y: 2, z: 4, core: 2. Of those that a mesh axis runs over, the one named last changes fastest.
Arguments:
- tokens: bfloat16 [4096, 2048], P(('grp', 'kv'), 'tp'), parts along dimension 0, may hold values from -5400 to 5400, as said below
- gain: bfloat16 [2048], replicated, may hold values from 0.099609375 to 1.8984375
- w_query: bfloat16 [2048, 1024], P(None, 'tp'), may hold values from -1 to 1
- w_key: bfloat16 [2048, 512], P(None, 'tp'), may hold values from -3 to 3
- w_value: bfloat16 [2048, 512], P(None, 'tp'), may hold values from -0.125 to 0.125
- w_out: bfloat16 [1024, 2048], P(None, 'tp'), may hold values from -2 to 2
- select: int32 [32, 32], P(('grp', 'kv')), parts along dimension 0, may hold values from -1 to 63, as said below
Outputs:
- mixed: bfloat16 [4096, 2048], P(('grp', 'kv'), 'tp'), parts along dimension 0
There are 2 independent parts, one for each index of `grp`. A program takes and returns all parts, laid end to end along the dimension named above; an argument that names none is the same for every part. Nothing has to cross between parts.
Inputs may be any that keep to these rules, and one draw needn't show every extreme that they name: Entries of tokens are finite with scales that vary by row and by column. `select`: row b lists distinct key blocks that start no later than query block b ends, or -1 for an empty slot. Every query block lists each key block of its own index of kv up to its own last position. Apart from its own index, the query blocks of one index of kv together list at most 2 distinct key blocks held by any other index; every index but the first lists exactly 2 blocks of the index before it.
All inputs are finite; a program needn't handle non-finite values.
Results may differ from a plain program's by a relative error of at most 0.012.
Values may be sent and summed in bfloat16 or wider, within the bound.
No kernel may reach another device: no remote copies, remote signals or barrier semaphores. Data moves between devices by JAX's collectives and lax.ppermute only.
A program may use at most 128 MiB of HBM per device.

v0:
```python
import jax
import jax.numpy as jnp
from jax import lax
from jax.sharding import PartitionSpec as P

HD = 128
QB = 128
KB = 32
CAP = 2


epsilon = 1e-06
theta = 10000.0


def rotary(values, positions):
    head_width = values.shape[-1]
    frequency = theta ** (-jnp.arange(0, head_width, 2, dtype=jnp.float32) / head_width)
    angles = positions.astype(jnp.float32)[:, None] * frequency[None, :]
    cosine = jnp.cos(angles)[:, None, :]
    sine_table = jnp.sin(angles)[:, None, :]
    front_half = values[..., : head_width // 2]
    second = values[..., head_width // 2 :]
    return jnp.concatenate(
        [front_half * cosine - second * sine_table, second * cosine + front_half * sine_table],
        axis=-1,
    )


def per_device(tokens, gain, w_query, w_key, w_value, w_out, select):
    tok_rows = tokens.shape[0]
    model_width = gain.shape[0]
    my_index = lax.axis_index("kv")
    kv_count = lax.axis_size("kv")
    kv_local = w_key.shape[1] // HD
    group_size = w_query.shape[1] // w_key.shape[1]
    gain_f32 = gain.astype(jnp.float32)
    piece_f32 = lax.all_gather(tokens, "tp", axis=1, tiled=True).astype(jnp.float32)
    scaled = (piece_f32 * gain_f32[None, :]).astype(jnp.bfloat16)
    acc_q = jnp.dot(scaled, w_query, preferred_element_type=jnp.float32)
    acc_k = jnp.dot(scaled, w_key, preferred_element_type=jnp.float32)
    acc_v = jnp.dot(scaled, w_value, preferred_element_type=jnp.float32)
    tokens_f32 = tokens.astype(jnp.float32)
    squares = lax.psum(jnp.sum(tokens_f32 * tokens_f32, axis=1), "tp")
    inverse = lax.rsqrt(squares / model_width + epsilon)[:, None]
    positions = my_index * tok_rows + jnp.arange(tok_rows, dtype=jnp.int32)
    queries = rotary((acc_q * inverse).reshape(tok_rows, -1, HD), positions).astype(jnp.bfloat16)
    keys_here = rotary((acc_k * inverse).reshape(tok_rows, kv_local, HD), positions).astype(
        jnp.bfloat16
    )
    values_here = (acc_v * inverse).astype(jnp.bfloat16).reshape(tok_rows, kv_local, HD)
    blocks_dev = tok_rows // KB
    key_blocks = keys_here.reshape(blocks_dev, KB, kv_local, HD)
    value_blocks = values_here.reshape(blocks_dev, KB, kv_local, HD)
    safe_ids = jnp.maximum(select, 0)
    flat_ids = select.reshape(-1)
    owner_of = jnp.where(flat_ids >= 0, flat_ids // blocks_dev, -1)
    peer_ids = jnp.arange(kv_count, dtype=jnp.int32)
    is_match = (owner_of[None, :] == peer_ids[:, None]) & (peer_ids[:, None] != my_index)
    ceiling = jnp.int32(1 << 30)
    lowest = jnp.min(jnp.where(is_match, flat_ids[None, :], ceiling), axis=1)
    highest = jnp.max(jnp.where(is_match, flat_ids[None, :], -1), axis=1)
    wanted = jnp.stack(
        [jnp.where(lowest < ceiling, lowest, -1), jnp.where(highest > lowest, highest, -1)], axis=1
    )
    asked_ids = lax.all_to_all(wanted, "kv", split_axis=0, concat_axis=0, tiled=True)
    local_index = jnp.clip(asked_ids - my_index * blocks_dev, 0, blocks_dev - 1)
    send_k = jnp.take(key_blocks, local_index, axis=0)
    send_v = jnp.take(value_blocks, local_index, axis=0)
    got_k, got_v = (
        lax.all_to_all(send_k, "kv", split_axis=0, concat_axis=0, tiled=True),
        lax.all_to_all(send_v, "kv", split_axis=0, concat_axis=0, tiled=True),
    )
    table_k = jnp.concatenate([key_blocks, got_k.reshape(-1, KB, kv_local, HD)], axis=0)
    table_v = jnp.concatenate([value_blocks, got_v.reshape(-1, KB, kv_local, HD)], axis=0)
    sel_owner = safe_ids // blocks_dev
    pair_ids = jnp.take(wanted, sel_owner, axis=0)
    slot_of = jnp.where(safe_ids == pair_ids[..., 0], 0, 1)
    table_index = jnp.where(
        sel_owner == my_index,
        safe_ids - my_index * blocks_dev,
        blocks_dev + sel_owner * CAP + slot_of,
    )
    query_blocks = select.shape[0]
    chosen_count = select.shape[1]
    keys_sel = jnp.take(table_k, table_index, axis=0).reshape(
        query_blocks, chosen_count * KB, kv_local, HD
    )
    values_sel = jnp.take(table_v, table_index, axis=0).reshape(
        query_blocks, chosen_count * KB, kv_local, HD
    )
    query_rows = queries.reshape(query_blocks, QB, kv_local, group_size, HD)
    scores = jnp.einsum(
        "bqgrd,bkgd->bgrqk", query_rows, keys_sel, preferred_element_type=jnp.float32
    ) * HD ** (-0.5)
    key_pos = (safe_ids[:, :, None] * KB + jnp.arange(KB, dtype=jnp.int32)[None, None, :]).reshape(
        query_blocks, -1
    )
    live_keys = jnp.repeat(select >= 0, KB, axis=1)
    q_pos = positions.reshape(query_blocks, QB)
    allowed = live_keys[:, None, :] & (key_pos[:, None, :] <= q_pos[:, :, None])
    scores = jnp.where(allowed[:, None, None], scores, -jnp.inf)
    row_max = jnp.max(scores, axis=-1, keepdims=True)
    raised = jnp.exp(scores - row_max)
    weights = (raised / jnp.sum(raised, axis=-1, keepdims=True)).astype(jnp.bfloat16)
    attended = jnp.einsum(
        "bgrqk,bkgd->bqgrd", weights, values_sel, preferred_element_type=jnp.float32
    )
    attended = attended.astype(jnp.bfloat16).reshape(tok_rows, -1)
    mixed = jnp.dot(
        lax.all_gather(attended, "tp", axis=1, tiled=True),
        w_out,
        preferred_element_type=jnp.float32,
    )
    return mixed.astype(jnp.bfloat16)


def solution(mesh):
    placed = (
        P(("grp", "kv"), "tp"),
        P(),
        P(None, "tp"),
        P(None, "tp"),
        P(None, "tp"),
        P(None, "tp"),
        P(("grp", "kv"), None),
    )
    return jax.shard_map(
        per_device, mesh=mesh, in_specs=placed, out_specs=P(("grp", "kv"), "tp"), check_vma=False
    )
```

profile of v0, /device:TPU:0, one launch (start us, length us, event | category | flops | bytes accessed | tf_op | source)
XLA Modules:
  0.0 91.5 jit_solution(3641176890367045859)
XLA Ops:
  6.5 0.7 all-gather.3.cloned.1.call-update
  7.3 0.8 reshape.334
  8.1 0.2 select_reduce_fusion.1
  8.2 0.1 copy.79
  8.3 0.1 copy.77
  8.4 0.7 pad_add_fusion
  9.1 6.3 %all-to-all-start = ((s32[4,1,2]{2,1,0:T(1,128)}), s32[4,1,2]{2,1,0:T(1,128)S(1)}, u32[]{:S(2)}, u32[]{:S(2)}) async-start(s32[4,1,2]{2,1,0:T(1,128)} %bitcast.31), calls=%async_computation | async-start | bytes 4096 | tf_op jit(solution)/shard_map/all_to_all | solution.py:66
  15.5 0.7 compare_and_fusion.3
  16.2 0.7 convert_element_type.52
  17.0 1.3 %gather_fusion = s32[128,2]{1,0:T(8,128)S(1)} fusion(s32[4,2]{1,0:T(4,128)} %pad_add_fusion, s32[1024]{0:T(1024)S(1)} %pad_clamp_fusion.2), kind=kCustom, calls=%fused_computation.4 | custom fusion | bytes 2560 | tf_op jit(solution)/shard_map/jit(_take)/gather | solution.py:77
  18.3 0.1 copy.104
  18.4 0.7 compare_and_fusion.1
  19.3 0.1 and.59
  19.4 0.7 maximum_multiply_fusion
  20.2 0.1 add.93
  20.3 1.2 %multiply_reduce_fusion = f32[512]{0:T(512)S(1)} fusion(bf16[512,512]{1,0:T(8,128)(2,1)} %param.11), kind=kLoop, calls=%fused_computation.26 | loop fusion | flops 785920 | bytes 526336 | tf_op jit(solution)/shard_map/reduce_sum | solution.py:44
  21.5 7.2 %psum.7 = f32[512]{0:T(512)S(1)} all-reduce(f32[512]{0:T(512)S(1)} %multiply_reduce_fusion), channel_id=1, replica_groups=mesh['grp'=2,'kv'=4,'tp'=4] {'tp'}, use_global_device_ids=true, to_apply=%region_1.0 | all-reduce | flops 512 | bytes 4096 | tf_op jit(solution)/shard_map/psum | solution.py:44
  28.8 0.5 multiply_cosine_fusion.1
  29.3 2.4 %compare_and_fusion = pred[4,128,1024]{1,2,0:T(8,128)(4,1)} fusion(s32[4,128]{1,0:T(4,128)S(1)} %add_add_fusion, s32[4,1024]{1,0:T(4,128)S(1)} %broadcast_add_fusion, pred[4,1024]{1,0:T(4,128)(4,1)S(1)} %and.59), kind=kLoop, calls=%fused_computation.14 | loop fusion | flops 1048576 | bytes 546816 | tf_op jit(solution)/shard_map/and | solution.py:101
  31.7 0.1 copy.85
  31.8 0.1 copy.86
  32.1 2.3 %all-gather.3.cloned.1.call-done = bf16[512,2048]{1,0:T(8,128)(2,1)} async-done(((bf16[512,512]{1,0:T(8,128)(2,1)}), bf16[512,2048]{1,0:T(8,128)(2,1)}) %all-gather.3.cloned.1.call-update) | async-done | bytes 2097168 | tf_op jit(solution)/shard_map/all_gather | solution.py:38
  34.3 2.5 %fusion.14 = f32[512,1,128]{2,0,1:T(8,128)S(1)} fusion(bf16[2048,128]{1,0:T(8,128)(2,1)} %param.14, bf16[512,2048]{1,0:T(8,128)(2,1)} %all-gather.3.cloned.1.call-done, f32[2048]{0:T(1024)S(1)} %convert_element_type.52, f32[512]{0:T(512)S(1)} %add_rsqrt_fusion), kind=kOutput, calls=%fused_computation.23 | convolution fusion | flops 271646720 | bytes 2893824 | tf_op jit(solution)/shard_map/dot_general | solution.py:41
  36.9 1.2 %fusion.24 = (bf16[512,1,64]{2,0,1:T(8,128)(2,1)S(1)}, bf16[512,1,64]{2,0,1:T(8,128)(2,1)S(1)}) fusion(f32[512,1,128]{2,0,1:T(8,128)S(1)} %fusion.14, f32[64]{0:T(128)S(1)} %multiply_power_fusion, f32[512]{0:T(512)S(1)} %add_convert_fusion.1), kind=kLoop, calls=%fused_computation.36 | loop fusion | flops 294912 | bytes 395520 | tf_op jit(solution)/shard_map/convert.7
  38.1 0.7 fusion.18
  38.9 0.6 gather_fusion.1
  39.4 0.1 maximum_bitcast_fusion.2
  39.5 0.6 gather_fusion.3
  40.1 0.7 broadcast_select_fusion.2
  40.8 4.6 %all-to-all-start.2 = ((bf16[4,2,32,1,128]{4,2,1,3,0:T(8,128)(2,1)}), bf16[4,2,32,1,128]{4,2,1,3,0:T(8,128)(2,1)S(1)}, u32[]{:S(2)}, u32[]{:S(2)}) async-start(bf16[4,2,32,1,128]{4,2,1,3,0:T(8,128)(2,1)} %get-tuple-element.26), calls=%async_computation.2 | async-start | bytes 131072 | tf_op jit(solution)/shard_map/all_to_all | solution.py:71
  45.5 2.4 %fusion.8 = f32[512,256]{0,1:T(8,128)S(1)} fusion(bf16[2048,256]{1,0:T(8,128)(2,1)S(1)} %copy-done.5, bf16[512,2048]{1,0:T(8,128)(2,1)} %all-gather.3.cloned.1.call-done, f32[2048]{0:T(1024)S(1)} %convert_element_type.52, f32[512]{0:T(512)S(1)} %add_rsqrt_fusion), kind=kOutput, calls=%fused_computation.19 | convolution fusion | flops 540147712 | bytes 3680256 | tf_op jit(solution)/shard_map/dot_general | solution.py:40
  48.0 0.9 copy.91
  48.9 0.9 copy.92
  49.8 1.5 %all-to-all-done.2 = bf16[4,2,32,1,128]{4,2,1,3,0:T(8,128)(2,1)S(1)} async-done(((bf16[4,2,32,1,128]{4,2,1,3,0:T(8,128)(2,1)}), bf16[4,2,32,1,128]{4,2,1,3,0:T(8,128)(2,1)S(1)}, u32[]{:S(2)}, u32[]{:S(2)}) %all-to-all-start.2) | async-done | bytes 65568 | tf_op jit(solution)/shard_map/all_to_all | solution.py:71
  51.2 3.6 %all-to-all-start.1 = ((bf16[4,2,32,1,128]{4,2,1,3,0:T(8,128)(2,1)}), bf16[4,2,32,1,128]{4,2,1,3,0:T(8,128)(2,1)S(1)}, u32[]{:S(2)}, u32[]{:S(2)}) async-start(bf16[4,2,32,1,128]{4,2,1,3,0:T(8,128)(2,1)} %get-tuple-element.27), calls=%async_computation.1 | async-start | bytes 131072 | tf_op jit(solution)/shard_map/all_to_all | solution.py:72
  54.9 0.1 maximum_bitcast_fusion.1
  55.0 5.6 %all-to-all-done.1 = bf16[4,2,32,1,128]{4,2,1,3,0:T(8,128)(2,1)S(1)} async-done(((bf16[4,2,32,1,128]{4,2,1,3,0:T(8,128)(2,1)}), bf16[4,2,32,1,128]{4,2,1,3,0:T(8,128)(2,1)S(1)}, u32[]{:S(2)}, u32[]{:S(2)}) %all-to-all-start.1) | async-done | bytes 65568 | tf_op jit(solution)/shard_map/all_to_all | solution.py:72
  60.6 0.8 gather_fusion.2
  61.4 0.8 gather_fusion.4
  62.2 0.3 broadcast_select_fusion
  62.5 0.7 copy-done.1
  63.3 0.8 fusion.1
  64.2 1.0 %fusion = f32[4,2,128]{2,1,0:T(2,128)S(1)} fusion(f32[4,1024,128,2]{2,1,3,0:T(8,128)S(1)} %get-tuple-element.29, f32[4,2,128]{2,1,0:T(2,128)S(1)} %get-tuple-element.28, pred[4,128,1024]{1,2,0:T(8,128)(4,1)S(1)} %copy-done.1), kind=kLoop, calls=%fused_computation.9 | loop fusion | flops 4193280 | bytes 4726784 | tf_op jit(solution)/shard_map/reduce_sum | solution.py:105
  65.1 1.4 %fusion.15 = bf16[4,128,1,2,128]{1,4,3,0,2:T(8,128)(2,1)S(1)} fusion(bf16[4,1024,128,1]{2,1,3,0:T(8,128)(2,1)S(1)} %bitcast.96, f32[4,2,128]{2,1,0:T(2,128)S(1)} %fusion, f32[4,2,128]{2,1,0:T(2,128)S(1)} %get-tuple-element.28, f32[4,1024,128,2]{2,1,3,0:T(8,128)S(1)} %get-tuple-element.29, pred[4,128,1024]{1,2,0:T(8,128)(4,1)S(1)} %copy-done.1), kind=kOutput, calls=%fused_computation.24 | convolution fusion | flops 273809408 | bytes 6037504 | tf_op jit(solution)/shard_map/bgrqk,bkgd->bqgrd/dot_general | solution.py:106
  66.5 0.2 copy.95
  66.7 0.7 copy.107
  67.4 14.5 %all-gather.5.cloned.1.call-done = bf16[512,1024]{1,0:T(8,128)(2,1)} async-done(((bf16[512,256]{1,0:T(8,128)(2,1)}), bf16[512,1024]{1,0:T(8,128)(2,1)}) %all-gather.5.cloned.1.call-update) | async-done | bytes 1048592 | tf_op jit(solution)/shard_map/all_gather | solution.py:111
  81.9 2.7 %convolution_convert_fusion = bf16[512,512]{1,0:T(8,128)(2,1)} fusion(bf16[512,1024]{1,0:T(8,128)(2,1)} %all-gather.5.cloned.1.call-done, bf16[1024,512]{1,0:T(8,128)(2,1)S(1)} %copy-done), kind=kOutput, calls=%fused_computation.18 | convolution fusion | flops 537133056 | bytes 2621440 | tf_op jit(solution)/shard_map/dot_general | solution.py:110
  (41 shorter events, 1.0 us)
Async XLA Ops:
  6.5 75.4 %copy-start = (bf16[1024,512]{1,0:T(8,128)(2,1)S(1)}, bf16[1024,512]{1,0:T(8,128)(2,1)}, u32[]{:S(2)}) copy-start(bf16[1024,512]{1,0:T(8,128)(2,1)} %param.16) | copy-start | bytes 3145732
  6.5 27.8 %all-gather.3.cloned.1.call-start = ((), (), s32[]{:S(2)}) async-start(), calls=%async_computation.3 | async-start | bytes 2621440 | tf_op jit(solution)/shard_map/all_gather | solution.py:38
  9.1 22.6 %all-to-all-start = ((s32[4,1,2]{2,1,0:T(1,128)}), s32[4,1,2]{2,1,0:T(1,128)S(1)}, u32[]{:S(2)}, u32[]{:S(2)}) async-start(s32[4,1,2]{2,1,0:T(1,128)} %bitcast.31), calls=%async_computation | async-start | bytes 4096 | tf_op jit(solution)/shard_map/all_to_all | solution.py:66
  32.1 13.4 %copy-start.5 = (bf16[2048,256]{1,0:T(8,128)(2,1)S(1)}, bf16[2048,256]{1,0:T(8,128)(2,1)}, u32[]{:S(2)}) copy-start(bf16[2048,256]{1,0:T(8,128)(2,1)} %param.13) | copy-start | bytes 3145732
  34.3 3.8 %copy-start.4 = (bf16[512,2048]{1,0:T(8,128)(2,1)S(1)}, bf16[512,2048]{1,0:T(8,128)(2,1)}, u32[]{:S(2)}) copy-start(bf16[512,2048]{1,0:T(8,128)(2,1)} %all-gather.3.cloned.1.call-done) | copy-start | bytes 6291460
  34.3 3.8 %copy-start.6 = (bf16[2048,128]{1,0:T(8,128)(2,1)S(1)}, bf16[2048,128]{1,0:T(8,128)(2,1)}, u32[]{:S(2)}) copy-start(bf16[2048,128]{1,0:T(8,128)(2,1)} %param.15) | copy-start | bytes 1572868
  40.8 10.4 %all-to-all-start.2 = ((bf16[4,2,32,1,128]{4,2,1,3,0:T(8,128)(2,1)}), bf16[4,2,32,1,128]{4,2,1,3,0:T(8,128)(2,1)S(1)}, u32[]{:S(2)}, u32[]{:S(2)}) async-start(bf16[4,2,32,1,128]{4,2,1,3,0:T(8,128)(2,1)} %get-tuple-element.26), calls=%async_computation.2 | async-start | bytes 131072 | tf_op jit(solution)/shard_map/all_to_all | solution.py:71
  51.2 9.4 %all-to-all-start.1 = ((bf16[4,2,32,1,128]{4,2,1,3,0:T(8,128)(2,1)}), bf16[4,2,32,1,128]{4,2,1,3,0:T(8,128)(2,1)S(1)}, u32[]{:S(2)}, u32[]{:S(2)}) async-start(bf16[4,2,32,1,128]{4,2,1,3,0:T(8,128)(2,1)} %get-tuple-element.27), calls=%async_computation.1 | async-start | bytes 131072 | tf_op jit(solution)/shard_map/all_to_all | solution.py:72
  54.9 27.1 %all-gather.5.cloned.1.call-start = ((), (), s32[]{:S(2)}) async-start(), calls=%async_computation.4 | async-start | bytes 1310720 | tf_op jit(solution)/shard_map/all_gather | solution.py:111
  62.2 1.0 %copy-start.1 = (pred[4,128,1024]{1,2,0:T(8,128)(4,1)S(1)}, pred[4,128,1024]{1,2,0:T(8,128)(4,1)}, u32[]{:S(2)}) copy-start(pred[4,128,1024]{1,2,0:T(8,128)(4,1)} %compare_and_fusion) | copy-start | bytes 1572868
  62.2 1.1 %copy-start.2 = (bf16[4,128,2,64]{3,1,2,0:T(8,128)(2,1)S(1)}, bf16[4,128,2,64]{3,1,2,0:T(8,128)(2,1)}, u32[]{:S(2)}) copy-start(bf16[4,128,2,64]{3,1,2,0:T(8,128)(2,1)} %copy.91) | copy-start | bytes 393220
  62.2 1.2 %copy-start.3 = (bf16[4,128,2,64]{3,1,2,0:T(8,128)(2,1)S(1)}, bf16[4,128,2,64]{3,1,2,0:T(8,128)(2,1)}, u32[]{:S(2)}) copy-start(bf16[4,128,2,64]{3,1,2,0:T(8,128)(2,1)} %copy.92) | copy-start | bytes 393220
Sparse Core Ops, SparseCore 0:
  8.9 25.4 all-gather.2
  67.6 14.3 all-gather.4
where the time goes:
time: 92.2 us; the launch traced here: 91.5 us
  waiting for transfers between devices  24.6 us (27%)
  starting transfers between devices  14.6 us (16%)
  between operations  13.6 us (15%)
  other arithmetic  11.4 us (12%)
  matrix products  10.5 us (11%)
  local copies, waits for them, and re-layouts  9.64 us (10%)
  blocking collectives  7.17 us (8%)
    all_gather x1, waiting for transfers between devices, per_device(): lax.all_gather(attended, 'tp', axis=1, tiled=True)  14.5 us
    psum x1, blocking collectives, per_device(): squares = lax.psum(jnp.sum(tokens_f32 * tokens_f32, axis=1), 'tp')  7.17 us
    all_to_all x1, starting transfers between devices, per_device(): lax.all_to_all(wanted, 'kv', split_axis=0, concat_axis=0, tiled=True)  6.35 us
    all_to_all x1, waiting for transfers between devices, per_device(): lax.all_to_all(send_v, 'kv', split_axis=0, concat_axis=0, tiled=True)  5.63 us
    all_to_all x1, starting transfers between devices, per_device(): lax.all_to_all(send_k, 'kv', split_axis=0, concat_axis=0, tiled=True)  4.65 us
    all_to_all x1, starting transfers between devices, per_device(): lax.all_to_all(send_v, 'kv', split_axis=0, concat_axis=0, tiled=True)  3.63 us
    dot_general x1, matrix products, per_device(): jnp.dot(lax.all_gather(attended, 'tp', axis=1, tiled=True), w_out, prefer...  2.73 us
    dot_general x1, matrix products, per_device(): acc_k = jnp.dot(scaled, w_key, preferred_element_type=jnp.float32)  2.54 us
  transfers between devices with their start and end apart: 5, of which 4 were waited for; matrix products, arithmetic and copies ran while one was open for 17% of the time, Pallas kernels for 0%

commit v1 on v0

v1 whole, which is shorter than its diff:
```python
import functools

import jax
import jax.numpy as jnp
from jax import lax
from jax.experimental import pallas as pl
from jax.experimental.pallas import tpu as pltpu
from jax.sharding import PartitionSpec as P

HD = 128
KB = 32
CAP = 2
LANES = 128
SUBLANES = 8

epsilon = 1e-06
theta = 10000.0

f32 = jnp.float32
bf16 = jnp.bfloat16

VMEM = pltpu.VMEM
SMEM = pltpu.SMEM


def vspec():
    return pl.BlockSpec(memory_space=VMEM)


def sspec():
    return pl.BlockSpec(memory_space=SMEM)


def swap(array, axis, mask):
    size = lax.axis_size(axis)
    return lax.ppermute(array, axis, [(i, i ^ mask) for i in range(size)])


def gather_pieces(array, axis):
    size = lax.axis_size(axis)
    pieces = {0: array}
    mask = size >> 1
    while mask:
        for known in sorted(pieces):
            if not known & (2 * mask - 1):
                pieces[known | mask] = swap(pieces[known], axis, mask)
        mask >>= 1
    return [pieces[k] for k in range(size)]


def request_kernel(info_ref, select_ref, *out_refs, kv_count, blocks_dev):
    *ask_refs, bias_ref = out_refs
    me = info_ref[1]
    listed = select_ref[...]
    query_blocks = listed.shape[0]
    lane = lax.broadcasted_iota(jnp.int32, (SUBLANES, LANES), 1)
    ceiling = jnp.int32(1 << 30)
    for shift in range(1, kv_count):
        first = (me - shift) * blocks_dev
        match = (listed >= 0) & (listed >= first) & (listed < first + blocks_dev)
        low = jnp.min(jnp.where(match, listed, ceiling))
        high = jnp.max(jnp.where(match, listed, -1))
        high = jnp.where(high > low, high, -1)
        low = jnp.where(low < ceiling, low, -1)
        ask_refs[shift - 1][...] = jnp.where(lane == 0, low, jnp.where(lane == 1, high, -1))
        bits = []
        for wanted in (low, high):
            hit = jnp.where((listed == wanted) & match, 1.0, 0.0)
            bits.append(jnp.max(hit, axis=1, keepdims=True))
        lane_here = lax.broadcasted_iota(jnp.int32, (query_blocks, CAP * KB), 1)
        hit = jnp.where(lane_here < KB, bits[0], bits[1])
        bias_ref[shift - 1] = jnp.where(hit > 0.5, 0.0, -jnp.inf)


def make_requests(info, select, kv_count, blocks_dev):
    shifts = max(kv_count - 1, 1)
    outs = [jax.ShapeDtypeStruct((SUBLANES, LANES), jnp.int32)] * (kv_count - 1)
    outs.append(jax.ShapeDtypeStruct((shifts, select.shape[0], CAP * KB), f32))
    return pl.pallas_call(
        functools.partial(request_kernel, kv_count=kv_count, blocks_dev=blocks_dev),
        out_shape=outs,
        in_specs=[sspec(), vspec()],
        out_specs=[vspec()] * len(outs),
        name="requests",
    )(info, select)


def project_kernel(info_ref, *refs, pieces, heads, row0):
    token_refs = refs[:pieces]
    gain_ref, wq_ref, wk_ref, wv_ref, cos_ref, sin_ref, q_ref, k_ref, v_ref = refs[pieces:]
    me = info_ref[0]
    rows, width = token_refs[0].shape
    step = min(rows, 128)
    for r in range(0, rows, step):
        squares = jnp.zeros((step, 1), f32)
        acc_q = jnp.zeros((step, wq_ref.shape[1]), f32)
        acc_kv = jnp.zeros((step, 2 * HD), f32)
        for k in range(pieces):
            origin = jnp.bitwise_xor(me, k)
            col = pl.multiple_of(origin * width, width)
            piece = token_refs[k][r : r + step, :].astype(f32)
            squares += jnp.sum(piece * piece, axis=1, keepdims=True)
            scaled = (piece * gain_ref[origin].astype(f32)).astype(bf16)
            acc_q += jnp.dot(scaled, wq_ref[pl.ds(col, width), :], preferred_element_type=f32)
            w_kv = jnp.concatenate([wk_ref[pl.ds(col, width), :], wv_ref[pl.ds(col, width), :]], axis=1)
            acc_kv += jnp.dot(scaled, w_kv, preferred_element_type=f32)
        inverse = lax.rsqrt(squares / (width * pieces) + epsilon)
        cos = cos_ref[row0 + r : row0 + r + step, :]
        sin = sin_ref[row0 + r : row0 + r + step, :]

        def rotate(x):
            return x * cos + pltpu.roll(x, HD // 2, 1) * sin

        for h in range(heads):
            head = acc_q[:, h * HD : (h + 1) * HD] * inverse
            q_ref[r : r + step, h * HD : (h + 1) * HD] = rotate(head).astype(bf16)
        k_ref[r : r + step, :] = rotate(acc_kv[:, :HD] * inverse).astype(bf16)
        v_ref[r : r + step, :] = (acc_kv[:, HD:] * inverse).astype(bf16)


def project(info, pieces, gain, wq, wk, wv, cos, sin, row0):
    rows = pieces[0].shape[0]
    outs = [
        jax.ShapeDtypeStruct((rows, wq.shape[1]), bf16),
        jax.ShapeDtypeStruct((rows, HD), bf16),
        jax.ShapeDtypeStruct((rows, HD), bf16),
    ]
    count = len(pieces)
    return pl.pallas_call(
        functools.partial(project_kernel, pieces=count, heads=wq.shape[1] // HD, row0=row0),
        out_shape=outs,
        in_specs=[sspec()] + [vspec()] * (count + 6),
        out_specs=[vspec()] * 3,
        cost_estimate=pl.CostEstimate(
            flops=2 * rows * wq.shape[0] * 4 * HD, transcendentals=0, bytes_accessed=6 << 20
        ),
        name="project",
    )(info, *pieces, gain, wq, wk, wv, cos, sin)


def send_kernel(info_ref, *refs, count, blocks_dev):
    asked_refs = refs[:count]
    k_ref, v_ref = refs[count : count + 2]
    out_refs = refs[count + 2 :]
    first = info_ref[1] * blocks_dev
    for n in range(count):
        for slot in range(CAP):
            block = jnp.clip(asked_refs[n][0, slot] - first, 0, blocks_dev - 1)
            row = pl.multiple_of(block * KB, KB)
            out_refs[n][slot * KB : (slot + 1) * KB, :HD] = k_ref[pl.ds(row, KB), :]
            out_refs[n][slot * KB : (slot + 1) * KB, HD:] = v_ref[pl.ds(row, KB), :]


def pick_blocks(info, asked, keys, values, blocks_dev):
    count = len(asked)
    outs = [jax.ShapeDtypeStruct((CAP * KB, 2 * HD), bf16)] * count
    return pl.pallas_call(
        functools.partial(send_kernel, count=count, blocks_dev=blocks_dev),
        out_shape=outs,
        in_specs=[sspec()] * (count + 1) + [vspec()] * 2,
        out_specs=[vspec()] * count,
        name="pick_blocks",
    )(info, *asked, keys, values)


def stack_heads(q_ref, row, rows, heads):
    return jnp.concatenate(
        [q_ref[row : row + rows, h * HD : (h + 1) * HD] for h in range(heads)], axis=0
    )


NT = (((1,), (1,)), ((), ()))


def local_kernel(q_ref, k_ref, v_ref, m_ref, l_ref, o_ref, *, query_rows, heads):
    scale = HD**-0.5
    stacked = heads * query_rows
    row_at = lax.broadcasted_iota(jnp.int32, (stacked, query_rows), 0) % query_rows
    col_at = lax.broadcasted_iota(jnp.int32, (stacked, query_rows), 1)
    causal = col_at <= row_at
    for b in range(q_ref.shape[0] // query_rows):
        q = stack_heads(q_ref, b * query_rows, query_rows, heads)
        parts = []
        for c in range(b + 1):
            s = lax.dot_general(
                q, k_ref[c * query_rows : (c + 1) * query_rows, :], NT, preferred_element_type=f32
            )
            s = s * scale
            parts.append(jnp.where(causal, s, -jnp.inf) if c == b else s)
        top = parts[0]
        for s in parts[1:]:
            top = jnp.maximum(top, s)
        m = jnp.max(top, axis=1, keepdims=True)
        total = jnp.zeros((stacked, query_rows), f32)
        out = jnp.zeros((stacked, HD), f32)
        for c, s in enumerate(parts):
            p = jnp.exp(s - m)
            total += p
            out += jnp.dot(
                p.astype(bf16), v_ref[c * query_rows : (c + 1) * query_rows, :], preferred_element_type=f32
            )
        m_ref[b] = jnp.broadcast_to(m, (stacked, LANES))
        l_ref[b] = jnp.broadcast_to(jnp.sum(total, axis=1, keepdims=True), (stacked, LANES))
        o_ref[b] = out


def attend_local(queries, keys, values, query_rows):
    rows, width = queries.shape
    heads = width // HD
    shape = jax.ShapeDtypeStruct((rows // query_rows, heads * query_rows, LANES), f32)
    return pl.pallas_call(
        functools.partial(local_kernel, query_rows=query_rows, heads=heads),
        out_shape=[shape] * 3,
        in_specs=[vspec()] * 3,
        out_specs=[vspec()] * 3,
        cost_estimate=pl.CostEstimate(
            flops=4 * rows * rows * width, transcendentals=rows * rows * heads, bytes_accessed=2 << 20
        ),
        name="attend_local",
    )(queries, keys, values)


def remote_kernel(q_ref, m_ref, l_ref, o_ref, bias_ref, *refs, query_rows, heads, block0, blocks, count):
    kv_refs = refs[:count]
    out_ref = refs[count]
    scale = HD**-0.5
    for b in range(block0, block0 + blocks):
        q = stack_heads(q_ref, b * query_rows, query_rows, heads)
        m1 = m_ref[b]
        parts = []
        m = m1[:, :1]
        for n in range(count):
            s = lax.dot_general(q, kv_refs[n][:, :HD], NT, preferred_element_type=f32)
            s = s * scale + bias_ref[n, b : b + 1, :]
            parts.append(s)
            m = jnp.maximum(m, jnp.max(s, axis=1, keepdims=True))
        shrink = jnp.exp(m1[:, :1] - m)
        total = l_ref[b][:, :1] * shrink
        out = o_ref[b] * shrink
        for n in range(count):
            p = jnp.exp(parts[n] - m)
            total += jnp.sum(p, axis=1, keepdims=True)
            out += jnp.dot(p.astype(bf16), kv_refs[n][:, HD:], preferred_element_type=f32)
        out = out / total
        for h in range(heads):
            row = (b - block0) * query_rows
            out_ref[row : row + query_rows, h * HD : (h + 1) * HD] = out[
                h * query_rows : (h + 1) * query_rows, :
            ].astype(bf16)


def attend_remote(queries, m, l, o, bias, received, query_rows, block0, blocks):
    heads = queries.shape[1] // HD
    count = len(received)
    return pl.pallas_call(
        functools.partial(
            remote_kernel,
            query_rows=query_rows,
            heads=heads,
            block0=block0,
            blocks=blocks,
            count=count,
        ),
        out_shape=jax.ShapeDtypeStruct((blocks * query_rows, heads * HD), bf16),
        in_specs=[vspec()] * (5 + count),
        out_specs=vspec(),
        name="attend_remote",
    )(queries, m, l, o, bias, *received)


def output_kernel(info_ref, *refs, pieces):
    att_refs = refs[:pieces]
    w_ref = refs[pieces]
    out_ref = refs[-1]
    me = info_ref[0]
    rows, width = att_refs[0].shape
    acc = jnp.zeros(out_ref.shape, f32)
    for k in range(pieces):
        row = pl.multiple_of(jnp.bitwise_xor(me, k) * width, width)
        acc += jnp.dot(att_refs[k][...], w_ref[pl.ds(row, width), :], preferred_element_type=f32)
    out_ref[...] = acc.astype(bf16)


def project_out(info, pieces, w_out, index, total_rows, so_far):
    rows = pieces[0].shape[0]
    count = len(pieces)
    args = [info, *pieces, w_out]
    specs = [sspec()] + [vspec()] * (count + 1)
    aliases = {}
    if so_far is not None:
        aliases = {len(args): 0}
        args.append(so_far)
        specs.append(pl.BlockSpec(memory_space=pl.ANY))
    return pl.pallas_call(
        functools.partial(output_kernel, pieces=count),
        grid=(1,),
        out_shape=jax.ShapeDtypeStruct((total_rows, w_out.shape[1]), bf16),
        in_specs=specs,
        out_specs=pl.BlockSpec((rows, w_out.shape[1]), lambda i: (index, 0)),
        input_output_aliases=aliases,
        cost_estimate=pl.CostEstimate(
            flops=2 * rows * w_out.shape[0] * w_out.shape[1], transcendentals=0, bytes_accessed=2 << 20
        ),
        name="project_out",
    )(*args)


def shift_up(array, axis, shift):
    size = lax.axis_size(axis)
    return lax.ppermute(array, axis, [(i, i + shift) for i in range(size - shift)])


def shift_down(array, axis, shift):
    size = lax.axis_size(axis)
    return lax.ppermute(array, axis, [(i, i - shift) for i in range(shift, size)])


def per_device(tokens, gain, w_query, w_key, w_value, w_out, select):
    tok_rows, width = tokens.shape
    kv_count = lax.axis_size("kv")
    tp_count = lax.axis_size("tp")
    tp_index = lax.axis_index("tp")
    kv_index = lax.axis_index("kv")
    blocks_dev = tok_rows // KB
    query_blocks = select.shape[0]
    query_rows = tok_rows // query_blocks
    info = jnp.stack([tp_index, kv_index]).astype(jnp.int32)

    pieces = gather_pieces(tokens, "tp")
    *asks, bias = make_requests(info, select, kv_count, blocks_dev)
    asked = [shift_down(asks[n], "kv", n + 1) for n in range(kv_count - 1)]

    half = HD // 2
    frequency = theta ** (-jnp.arange(0, HD, 2, dtype=f32) / HD)
    positions = kv_index * tok_rows + jnp.arange(tok_rows, dtype=jnp.int32)
    angles = positions.astype(f32)[:, None] * frequency[None, :]
    cos, sin = jnp.cos(angles), jnp.sin(angles)
    cos = jnp.concatenate([cos, cos], axis=1)
    sin = jnp.concatenate([-sin, sin], axis=1)

    gain_rows = gain.reshape(tp_count, 1, width)
    queries, keys, values = project(info, pieces, gain_rows, w_query, w_key, w_value, cos, sin, 0)
    received = []
    if kv_count > 1:
        sends = pick_blocks(info, asked, keys, values, blocks_dev)
        received = [shift_up(sends[n], "kv", n + 1) for n in range(kv_count - 1)]
    m, l, o = attend_local(queries, keys, values, query_rows)
    parts = 2 if query_blocks % 2 == 0 else 1
    blocks = query_blocks // parts
    mixed = None
    for part in range(parts):
        att = attend_remote(queries, m, l, o, bias, received, query_rows, part * blocks, blocks)
        att_pieces = gather_pieces(att, "tp")
        mixed = project_out(info, att_pieces, w_out, part, tok_rows, mixed)
    return mixed


def solution(mesh):
    placed = (
        P(("grp", "kv"), "tp"),
        P(),
        P(None, "tp"),
        P(None, "tp"),
        P(None, "tp"),
        P(None, "tp"),
        P(("grp", "kv"), None),
    )
    return jax.shard_map(
        per_device, mesh=mesh, in_specs=placed, out_specs=P(("grp", "kv"), "tp"), check_vma=False
    )
```

time: 92.2 us -> 61 us (0.66)
  Pallas kernels: 0 us -> 23.2 us
  waiting for transfers between devices: 24.6 us -> 10.2 us
  between operations: 13.6 us -> 0.22 us
  matrix products: 10.5 us -> 0 us
  other arithmetic: 11.4 us -> 2.62 us
  blocking collectives: 7.17 us -> 0 us
  starting transfers between devices: 14.6 us -> 19 us
  local copies, waits for them, and re-layouts: 9.64 us -> 5.41 us
    pallas_call x0 -> x8, Pallas kernels: none -> 23.2 us  [the longest x2 6.65 us: attend_remote(): pl.pallas_call(functools.partial(remote_kernel, query_rows=query_rows, he...]
    ppermute x0 -> x15, starting transfers between devices: none -> 19 us  [the longest x3 9.51 us: shift_up(): lax.ppermute(array, axis, [(i, i + shift) for i in range(size - shift)])]
    all_gather x2 -> x0, waiting for transfers between devices: 16.8 us -> none  [the longest x1 14.5 us: per_device(): lax.all_gather(attended, 'tp', axis=1, tiled=True)]
    all_to_all x3 -> x0, starting transfers between devices: 14.6 us -> none  [the longest x1 6.35 us: per_device(): lax.all_to_all(wanted, 'kv', split_axis=0, concat_axis=0, tiled=True)]
    dot_general x6 -> x0, matrix products: 10.5 us -> none  [the longest x1 2.73 us: per_device(): jnp.dot(lax.all_gather(attended, 'tp', axis=1, tiled=True), w_out, prefer...]
    ppermute x0 -> x15, waiting for transfers between devices: none -> 10.2 us  [the longest x9 10.1 us: swap(): return lax.ppermute(array, axis, [(i, i ^ mask) for i in range(size)])]
    psum x1 -> x0, blocking collectives: 7.17 us -> none  [per_device(): squares = lax.psum(jnp.sum(tokens_f32 * tokens_f32, axis=1), 'tp')]
    all_to_all x3 -> x0, waiting for transfers between devices: 7.09 us -> none  [the longest x1 5.63 us: per_device(): lax.all_to_all(send_v, 'kv', split_axis=0, concat_axis=0, tiled=True)]
  transfers between devices with their start and end apart: 5 -> 15, of which waited for: 4 -> 3; matrix products, arithmetic and copies ran while one was open for 17% -> 5% of each run, Pallas kernels for 0% -> 26%
where the time goes in v1:
time: 61 us; the launch traced here: 60.6 us
  Pallas kernels  23.2 us (38%)
  starting transfers between devices  19 us (31%)
  waiting for transfers between devices  10.2 us (17%)
  local copies, waits for them, and re-layouts  5.41 us (9%)
  other arithmetic  2.62 us (4%)
    ppermute x9, waiting for transfers between devices, swap(): return lax.ppermute(array, axis, [(i, i ^ mask) for i in range(size)])  10.1 us
    ppermute x3, starting transfers between devices, shift_up(): lax.ppermute(array, axis, [(i, i + shift) for i in range(size - shift)])  9.51 us
    pallas_call x2, Pallas kernels, attend_remote(): pl.pallas_call(functools.partial(remote_kernel, query_rows=query_rows, he...  6.65 us
    ppermute x9, starting transfers between devices, swap(): return lax.ppermute(array, axis, [(i, i ^ mask) for i in range(size)])  5.51 us
    pallas_call x2, Pallas kernels, project_out(): pl.pallas_call(functools.partial(output_kernel, pieces=count), grid=(1,),...  5.29 us
    pallas_call x1, Pallas kernels, project(): pl.pallas_call(functools.partial(project_kernel, pieces=count, heads=wq.s...  4.86 us
    unnamed x34, local copies, waits for them, and re-layouts  4.75 us
    ppermute x3, starting transfers between devices, shift_down(): lax.ppermute(array, axis, [(i, i - shift) for i in range(shift, size)])  4 us
  transfers between devices with their start and end apart: 15, of which 3 were waited for; matrix products, arithmetic and copies ran while one was open for 5% of the time, Pallas kernels for 26%

profile of v1, /device:TPU:0, one launch (start us, length us, event | category | flops | bytes accessed | tf_op | source)
XLA Modules:
  0.0 60.6 jit_solution(12377600008641975086)
XLA Ops:
  0.0 3.0 %collective-permute-start.1 = (bf16[512,512]{1,0:T(8,128)(2,1)}, bf16[512,512]{1,0:T(8,128)(2,1)S(1)}, u32[]{:S(2)}, u32[]{:S(2)}) collective-permute-start(bf16[512,512]{1,0:T(8,128)(2,1)} %refs_0_.1), channel_id=1, source_target_pairs={{0,2},{1,3},{2,0},{3,1},{4,6},{5,7},{6,4},{7,5},{8,10},{9,11},{10,... | collective-permute-start | bytes 1572872 | tf_op jit(solution)/shard_map/ppermute | solution.py:36
  3.0 0.0 collective-permute-start
  3.0 0.6 pad_add_fusion.info_ref
  3.6 1.6 %requests.1 = (s32[8,128]{1,0:T(8,128)}, s32[8,128]{1,0:T(8,128)}, s32[8,128]{1,0:T(8,128)}, f32[3,4,64]{2,1,0:T(4,128)}) custom-call(s32[2]{0:T(128)} %pad_add_fusion.info_ref, s32[4,32]{1,0:T(4,128)} %select_ref.1), custom_call_target="tpu_custom_call" | custom-call | tf_op jit(solution)/shard_map/requests/pallas_call | solution.py:79
  5.1 1.4 %collective-permute-start.3 = (s32[8,128]{1,0:T(8,128)}, s32[8,128]{1,0:T(8,128)S(1)}, u32[]{:S(2)}, u32[]{:S(2)}) collective-permute-start(s32[8,128]{1,0:T(8,128)} %get-tuple-element.25), channel_id=1, source_target_pairs={{4,0},{8,4},{12,8},{5,1},{9,5},{13,9},{6,2},{10,6},{14,10},{7,3},{... | collective-permute-start | bytes 12296 | tf_op jit(solution)/shard_map/ppermute | solution.py:315
  6.6 1.3 %collective-permute-start.4 = (s32[8,128]{1,0:T(8,128)}, s32[8,128]{1,0:T(8,128)S(1)}, u32[]{:S(2)}, u32[]{:S(2)}) collective-permute-start(s32[8,128]{1,0:T(8,128)} %get-tuple-element.26), channel_id=1, source_target_pairs={{8,0},{12,4},{9,1},{13,5},{10,2},{14,6},{11,3},{15,7},{24,16},{28,... | collective-permute-start | bytes 12296 | tf_op jit(solution)/shard_map/ppermute | solution.py:315
  7.9 1.3 %collective-permute-start.5 = (s32[8,128]{1,0:T(8,128)}, s32[8,128]{1,0:T(8,128)S(1)}, u32[]{:S(2)}, u32[]{:S(2)}) collective-permute-start(s32[8,128]{1,0:T(8,128)} %get-tuple-element.27), channel_id=1, source_target_pairs={{12,0},{13,1},{14,2},{15,3},{28,16},{29,17},{30,18},{31,19}} | collective-permute-start | bytes 12296 | tf_op jit(solution)/shard_map/ppermute | solution.py:315
  9.2 5.9 %collective-permute-done.1.refs_2_ = bf16[512,512]{1,0:T(8,128)(2,1)S(1)} collective-permute-done((bf16[512,512]{1,0:T(8,128)(2,1)}, bf16[512,512]{1,0:T(8,128)(2,1)S(1)}, u32[]{:S(2)}, u32[]{:S(2)}) %collective-permute-start.1) | collective-permute-done | bytes 524320 | tf_op jit(solution)/shard_map/ppermute | solution.py:36
  15.1 0.0 collective-permute-start.2
  15.1 0.7 %reshape.16.refs_4_ = bf16[4,1,512]{2,1,0:T(2,128)(2,1)} reshape(bf16[2048]{0:T(1024)(128)(2,1)S(1)} %copy-done.16) | data formatting | bytes 8192 | tf_op jit(solution)/shard_map/reshape | solution.py:341
  15.8 1.0 %fusion = (f32[512,64]{1,0:T(8,128)S(1)}, f32[512,64]{1,0:T(8,128)S(1)}, f32[512,64]{1,0:T(8,128)S(1)}) fusion(f32[64]{0:T(128)S(1)} %multiply_power_fusion, f32[512]{0:T(512)S(1)} %add_convert_fusion), kind=kLoop, calls=%fused_computation.4 | loop fusion | flops 65536 | bytes 395520 | tf_op jit(solution)/shard_map/neg | solution.py:339
  16.8 1.0 %pad_maximum_fusion = (f32[512,128]{1,0:T(8,128)}, f32[512,128]{1,0:T(8,128)}) fusion(f32[512,64]{1,0:T(8,128)S(1)} %get-tuple-element.33, f32[512,64]{1,0:T(8,128)S(1)} %get-tuple-element.32, f32[512,64]{1,0:T(8,128)S(1)} %get-tuple-element.31), kind=kLoop, calls=%fused_computation.2 | loop fusion | flops 131072 | bytes 917504 | tf_op jit(solution)/shard_map/concatenate | solution.py:338
  17.8 0.0 collective-permute-done.refs_1_
  17.8 0.0 collective-permute-done.2.refs_3_
  17.8 0.8 %copy-done.1 = bf16[512,512]{1,0:T(8,128)(2,1)} copy-done((bf16[512,512]{1,0:T(8,128)(2,1)}, bf16[512,512]{1,0:T(8,128)(2,1)S(1)}, u32[]{:S(2)}) %copy-start.1) | copy-done | bytes 524312
  18.6 0.2 copy-done.2
  18.8 4.9 %project.1 = (bf16[512,256]{1,0:T(8,128)(2,1)}, bf16[512,128]{1,0:T(8,128)(2,1)}, bf16[512,128]{1,0:T(8,128)(2,1)}) custom-call(s32[2]{0:T(128)} %pad_add_fusion.info_ref, bf16[512,512]{1,0:T(8,128)(2,1)} %refs_0_.1, bf16[512,512]{1,0:T(8,128)(2,1)} %copy-done.1, bf16[512,512]{1,0:T(8,128)(2,1)} %copy-done, bf16[512,512]{1,0:T(8,128)(2,1)} %copy-done.2, ...), custom_call_target="tpu_custom_call" | custom-call | flops 1073741824 | bytes 6291456 | tf_op jit(solution)/shard_map/project/pallas_call | solution.py:129
  23.7 0.0 collective-permute-done.3.refs_0_
  23.7 0.0 copy-start.13
  23.7 0.0 collective-permute-done.4.refs_1_
  23.7 0.5 copy-done.13
  24.3 0.0 copy-done.14
  24.3 0.0 copy-done.15
  24.3 1.6 %pick_blocks.1 = (bf16[64,256]{1,0:T(8,128)(2,1)}, bf16[64,256]{1,0:T(8,128)(2,1)}, bf16[64,256]{1,0:T(8,128)(2,1)}) custom-call(s32[2]{0:T(128)} %pad_add_fusion.info_ref, s32[8,128]{1,0:T(8,128)} %copy-done.13, s32[8,128]{1,0:T(8,128)} %copy-done.14, s32[8,128]{1,0:T(8,128)} %copy-done.15, bf16[512,128]{1,0:T(8,128)(2,1)} %get-tuple-element.19.k_ref.refs_3_, ...), custom_call_target="tpu_custom_call" | custom-call | tf_op jit(solution)/shard_map/pick_blocks/pallas_call | solution.py:157
  25.9 3.7 %collective-permute-start.6 = (bf16[64,256]{1,0:T(8,128)(2,1)}, bf16[64,256]{1,0:T(8,128)(2,1)S(1)}, u32[]{:S(2)}, u32[]{:S(2)}) collective-permute-start(bf16[64,256]{1,0:T(8,128)(2,1)} %get-tuple-element.28), channel_id=1, source_target_pairs={{0,4},{4,8},{8,12},{1,5},{5,9},{9,13},{2,6},{6,10},{10,14},{3,7},{... | collective-permute-start | bytes 98312 | tf_op jit(solution)/shard_map/ppermute | solution.py:310
  29.7 4.5 %collective-permute-start.7 = (bf16[64,256]{1,0:T(8,128)(2,1)}, bf16[64,256]{1,0:T(8,128)(2,1)S(1)}, u32[]{:S(2)}, u32[]{:S(2)}) collective-permute-start(bf16[64,256]{1,0:T(8,128)(2,1)} %get-tuple-element.29), channel_id=1, source_target_pairs={{0,8},{4,12},{1,9},{5,13},{2,10},{6,14},{3,11},{7,15},{16,24},{20,... | collective-permute-start | bytes 98312 | tf_op jit(solution)/shard_map/ppermute | solution.py:310
  34.2 1.3 %collective-permute-start.8 = (bf16[64,256]{1,0:T(8,128)(2,1)}, bf16[64,256]{1,0:T(8,128)(2,1)S(1)}, u32[]{:S(2)}, u32[]{:S(2)}) collective-permute-start(bf16[64,256]{1,0:T(8,128)(2,1)} %get-tuple-element.30), channel_id=1, source_target_pairs={{0,12},{1,13},{2,14},{3,15},{16,28},{17,29},{18,30},{19,31}} | collective-permute-start | bytes 98312 | tf_op jit(solution)/shard_map/ppermute | solution.py:310
  35.5 3.2 %attend_local.1 = (f32[4,256,128]{2,1,0:T(8,128)}, f32[4,256,128]{2,1,0:T(8,128)}, f32[4,256,128]{2,1,0:T(8,128)}) custom-call(bf16[512,256]{1,0:T(8,128)(2,1)} %get-tuple-element.18.q_ref, bf16[512,128]{1,0:T(8,128)(2,1)} %get-tuple-element.19.k_ref.refs_3_, bf16[512,128]{1,0:T(8,128)(2,1)} %get-tuple-element.20.v_ref.refs_4_), custom_call_target="tpu_custom_call" | custom-call | flops 268435456 | bytes 2097152 | tf_op jit(solution)/shard_map/attend_local/pallas_call | solution.py:211
  38.7 0.0 collective-permute-done.8.refs_2_
  38.7 0.6 copy-done.4
  39.2 0.0 copy-done.5
  39.3 0.0 copy-done.6
  39.3 3.3 %attend_remote.3.refs_0_ = bf16[256,256]{1,0:T(8,128)(2,1)} custom-call(bf16[512,256]{1,0:T(8,128)(2,1)} %get-tuple-element.18.q_ref, f32[4,256,128]{2,1,0:T(8,128)} %get-tuple-element.21.m_ref, f32[4,256,128]{2,1,0:T(8,128)} %get-tuple-element.22.l_ref, f32[4,256,128]{2,1,0:T(8,128)} %get-tuple-element.23.o_ref, f32[3,4,64]{2,1,0:T(4,128)} %get-tuple-element.24.bias_ref, ...), custom_call_target="tpu_custom_call" | custom-call | tf_op jit(solution)/shard_map/attend_remote/pallas_call | solution.py:255
  42.6 1.5 %collective-permute-start.13 = (bf16[256,256]{1,0:T(8,128)(2,1)}, bf16[256,256]{1,0:T(8,128)(2,1)S(1)}, u32[]{:S(2)}, u32[]{:S(2)}) collective-permute-start(bf16[256,256]{1,0:T(8,128)(2,1)} %attend_remote.3.refs_0_), channel_id=1, source_target_pairs={{0,2},{1,3},{2,0},{3,1},{4,6},{5,7},{6,4},{7,5},{8,10},{9,11},{10,... | collective-permute-start | bytes 393224 | tf_op jit(solution)/shard_map/ppermute | solution.py:36
  44.1 3.3 %attend_remote.2.refs_0_ = bf16[256,256]{1,0:T(8,128)(2,1)} custom-call(bf16[512,256]{1,0:T(8,128)(2,1)} %get-tuple-element.18.q_ref, f32[4,256,128]{2,1,0:T(8,128)} %get-tuple-element.21.m_ref, f32[4,256,128]{2,1,0:T(8,128)} %get-tuple-element.22.l_ref, f32[4,256,128]{2,1,0:T(8,128)} %get-tuple-element.23.o_ref, f32[3,4,64]{2,1,0:T(4,128)} %get-tuple-element.24.bias_ref, ...), custom_call_target="tpu_custom_call" | custom-call | tf_op jit(solution)/shard_map/attend_remote/pallas_call | solution.py:255
  47.4 0.5 collective-permute-start.10
  48.0 0.0 collective-permute-start.12
  48.0 0.2 collective-permute-done.13.refs_2_
  48.1 0.4 collective-permute-start.14
  48.5 0.2 collective-permute-start.9
  48.6 4.0 %collective-permute-done.10.refs_2_ = bf16[256,256]{1,0:T(8,128)(2,1)S(1)} collective-permute-done((bf16[256,256]{1,0:T(8,128)(2,1)}, bf16[256,256]{1,0:T(8,128)(2,1)S(1)}, u32[]{:S(2)}, u32[]{:S(2)}) %collective-permute-start.10) | collective-permute-done | bytes 131104 | tf_op jit(solution)/shard_map/ppermute | solution.py:36
  52.7 0.0 collective-permute-done.14.refs_3_
  52.7 0.7 %copy-done.10 = bf16[256,256]{1,0:T(8,128)(2,1)} copy-done((bf16[256,256]{1,0:T(8,128)(2,1)}, bf16[256,256]{1,0:T(8,128)(2,1)S(1)}, u32[]{:S(2)}) %copy-start.10) | copy-done | bytes 131096
  53.4 0.7 %copy-done.12 = bf16[256,256]{1,0:T(8,128)(2,1)} copy-done((bf16[256,256]{1,0:T(8,128)(2,1)}, bf16[256,256]{1,0:T(8,128)(2,1)S(1)}, u32[]{:S(2)}) %copy-start.12) | copy-done | bytes 131096
  54.0 2.6 %project_out.2.refs_5_ = bf16[512,512]{1,0:T(8,128)(2,1)} custom-call(s32[2]{0:T(128)} %pad_add_fusion.info_ref, bf16[256,256]{1,0:T(8,128)(2,1)} %attend_remote.3.refs_0_, bf16[256,256]{1,0:T(8,128)(2,1)} %copy-done.10, bf16[256,256]{1,0:T(8,128)(2,1)} %copy-done.7, bf16[256,256]{1,0:T(8,128)(2,1)} %copy-done.12, bf16[1024,512]{1,0:T(8,128)(2,1)} %refs_4_.3), custom_call_target="tpu_custom_call" | custom-call | flops 268435456 | bytes 2097152 | tf_op jit(solution)/shard_map/project_out/pallas_call | solution.py:294
  56.7 0.6 %copy-done.9 = bf16[256,256]{1,0:T(8,128)(2,1)} copy-done((bf16[256,256]{1,0:T(8,128)(2,1)}, bf16[256,256]{1,0:T(8,128)(2,1)S(1)}, u32[]{:S(2)}) %copy-start.9) | copy-done | bytes 131096
  57.3 0.7 %copy-done.11 = bf16[256,256]{1,0:T(8,128)(2,1)} copy-done((bf16[256,256]{1,0:T(8,128)(2,1)}, bf16[256,256]{1,0:T(8,128)(2,1)S(1)}, u32[]{:S(2)}) %copy-start.11) | copy-done | bytes 131096
  58.0 2.6 %project_out.3 = bf16[512,512]{1,0:T(8,128)(2,1)} custom-call(s32[2]{0:T(128)} %pad_add_fusion.info_ref, bf16[256,256]{1,0:T(8,128)(2,1)} %attend_remote.2.refs_0_, bf16[256,256]{1,0:T(8,128)(2,1)} %copy-done.9, bf16[256,256]{1,0:T(8,128)(2,1)} %copy-done.8, bf16[256,256]{1,0:T(8,128)(2,1)} %copy-done.11, ...), custom_call_target="tpu_custom_call", output_to_operand_aliasing={{}: (6, {})} | custom-call | flops 268435456 | bytes 2097152 | tf_op jit(solution)/shard_map/project_out/pallas_call | solution.py:294
  (30 shorter events, 0.1 us)
Async XLA Ops:
  0.0 15.1 %collective-permute-start.1 = (bf16[512,512]{1,0:T(8,128)(2,1)}, bf16[512,512]{1,0:T(8,128)(2,1)S(1)}, u32[]{:S(2)}, u32[]{:S(2)}) collective-permute-start(bf16[512,512]{1,0:T(8,128)(2,1)} %refs_0_.1), channel_id=1, source_target_pairs={{0,2},{1,3},{2,0},{3,1},{4,6},{5,7},{6,4},{7,5},{8,10},{9,11},{10,... | collective-permute-start | bytes 1572872 | tf_op jit(solution)/shard_map/ppermute | solution.py:36
  3.0 14.9 %collective-permute-start = (bf16[512,512]{1,0:T(8,128)(2,1)}, bf16[512,512]{1,0:T(8,128)(2,1)S(1)}, u32[]{:S(2)}, u32[]{:S(2)}) collective-permute-start(bf16[512,512]{1,0:T(8,128)(2,1)} %refs_0_.1), channel_id=1, source_target_pairs={{0,1},{1,0},{2,3},{3,2},{4,5},{5,4},{6,7},{7,6},{8,9},{9,8},{10,11... | collective-permute-start | bytes 1572872 | tf_op jit(solution)/shard_map/ppermute | solution.py:36
  5.1 10.0 %copy-start.16 = (bf16[2048]{0:T(1024)(128)(2,1)S(1)}, bf16[2048]{0:T(1024)(128)(2,1)}, u32[]{:S(2)}) copy-start(bf16[2048]{0:T(1024)(128)(2,1)} %param.8) | copy-start | bytes 12292
  5.1 18.5 %collective-permute-start.3 = (s32[8,128]{1,0:T(8,128)}, s32[8,128]{1,0:T(8,128)S(1)}, u32[]{:S(2)}, u32[]{:S(2)}) collective-permute-start(s32[8,128]{1,0:T(8,128)} %get-tuple-element.25), channel_id=1, source_target_pairs={{4,0},{8,4},{12,8},{5,1},{9,5},{13,9},{6,2},{10,6},{14,10},{7,3},{... | collective-permute-start | bytes 12296 | tf_op jit(solution)/shard_map/ppermute | solution.py:315
  6.6 17.1 %collective-permute-start.4 = (s32[8,128]{1,0:T(8,128)}, s32[8,128]{1,0:T(8,128)S(1)}, u32[]{:S(2)}, u32[]{:S(2)}) collective-permute-start(s32[8,128]{1,0:T(8,128)} %get-tuple-element.26), channel_id=1, source_target_pairs={{8,0},{12,4},{9,1},{13,5},{10,2},{14,6},{11,3},{15,7},{24,16},{28,... | collective-permute-start | bytes 12296 | tf_op jit(solution)/shard_map/ppermute | solution.py:315
  7.9 15.8 %collective-permute-start.5 = (s32[8,128]{1,0:T(8,128)}, s32[8,128]{1,0:T(8,128)S(1)}, u32[]{:S(2)}, u32[]{:S(2)}) collective-permute-start(s32[8,128]{1,0:T(8,128)} %get-tuple-element.27), channel_id=1, source_target_pairs={{12,0},{13,1},{14,2},{15,3},{28,16},{29,17},{30,18},{31,19}} | collective-permute-start | bytes 12296 | tf_op jit(solution)/shard_map/ppermute | solution.py:315
  15.1 2.7 %copy-start = (bf16[512,512]{1,0:T(8,128)(2,1)}, bf16[512,512]{1,0:T(8,128)(2,1)S(1)}, u32[]{:S(2)}) copy-start(bf16[512,512]{1,0:T(8,128)(2,1)S(1)} %collective-permute-done.1.refs_2_) | copy-start | bytes 1572868
  15.1 2.7 %collective-permute-start.2 = (bf16[512,512]{1,0:T(8,128)(2,1)S(1)}, bf16[512,512]{1,0:T(8,128)(2,1)S(1)}, u32[]{:S(2)}, u32[]{:S(2)}) collective-permute-start(bf16[512,512]{1,0:T(8,128)(2,1)S(1)} %collective-permute-done.1.refs_2_), channel_id=1, source_target_pairs={{0,1},{1,0},{2,3},{3,2},{4,5},{5,4},{6,7},{7,6},{8,9},{9,8},{10,11... | collective-permute-start | bytes 1572872 | tf_op jit(solution)/shard_map/ppermute | solution.py:36
  17.8 0.8 %copy-start.1 = (bf16[512,512]{1,0:T(8,128)(2,1)}, bf16[512,512]{1,0:T(8,128)(2,1)S(1)}, u32[]{:S(2)}) copy-start(bf16[512,512]{1,0:T(8,128)(2,1)S(1)} %collective-permute-done.refs_1_) | copy-start | bytes 1572868
  17.8 1.0 %copy-start.2 = (bf16[512,512]{1,0:T(8,128)(2,1)}, bf16[512,512]{1,0:T(8,128)(2,1)S(1)}, u32[]{:S(2)}) copy-start(bf16[512,512]{1,0:T(8,128)(2,1)S(1)} %collective-permute-done.2.refs_3_) | copy-start | bytes 1572868
  23.7 0.6 copy-start.13
  23.7 0.6 copy-start.14
  23.7 0.6 copy-start.15
  25.9 12.7 %collective-permute-start.6 = (bf16[64,256]{1,0:T(8,128)(2,1)}, bf16[64,256]{1,0:T(8,128)(2,1)S(1)}, u32[]{:S(2)}, u32[]{:S(2)}) collective-permute-start(bf16[64,256]{1,0:T(8,128)(2,1)} %get-tuple-element.28), channel_id=1, source_target_pairs={{0,4},{4,8},{8,12},{1,5},{5,9},{9,13},{2,6},{6,10},{10,14},{3,7},{... | collective-permute-start | bytes 98312 | tf_op jit(solution)/shard_map/ppermute | solution.py:310
  29.7 9.0 %collective-permute-start.7 = (bf16[64,256]{1,0:T(8,128)(2,1)}, bf16[64,256]{1,0:T(8,128)(2,1)S(1)}, u32[]{:S(2)}, u32[]{:S(2)}) collective-permute-start(bf16[64,256]{1,0:T(8,128)(2,1)} %get-tuple-element.29), channel_id=1, source_target_pairs={{0,8},{4,12},{1,9},{5,13},{2,10},{6,14},{3,11},{7,15},{16,24},{20,... | collective-permute-start | bytes 98312 | tf_op jit(solution)/shard_map/ppermute | solution.py:310
  34.2 4.5 %collective-permute-start.8 = (bf16[64,256]{1,0:T(8,128)(2,1)}, bf16[64,256]{1,0:T(8,128)(2,1)S(1)}, u32[]{:S(2)}, u32[]{:S(2)}) collective-permute-start(bf16[64,256]{1,0:T(8,128)(2,1)} %get-tuple-element.30), channel_id=1, source_target_pairs={{0,12},{1,13},{2,14},{3,15},{16,28},{17,29},{18,30},{19,31}} | collective-permute-start | bytes 98312 | tf_op jit(solution)/shard_map/ppermute | solution.py:310
  38.6 0.6 copy-start.4
  38.6 0.6 %copy-start.5 = (bf16[64,256]{1,0:T(8,128)(2,1)}, bf16[64,256]{1,0:T(8,128)(2,1)S(1)}, u32[]{:S(2)}) copy-start(bf16[64,256]{1,0:T(8,128)(2,1)S(1)} %collective-permute-done.7.refs_1_) | copy-start | bytes 98308
  38.7 0.6 %copy-start.6 = (bf16[64,256]{1,0:T(8,128)(2,1)}, bf16[64,256]{1,0:T(8,128)(2,1)S(1)}, u32[]{:S(2)}) copy-start(bf16[64,256]{1,0:T(8,128)(2,1)S(1)} %collective-permute-done.8.refs_2_) | copy-start | bytes 98308
  42.6 5.4 %copy-start.3 = (bf16[256,256]{1,0:T(8,128)(2,1)S(1)}, bf16[256,256]{1,0:T(8,128)(2,1)}, u32[]{:S(2)}) copy-start(bf16[256,256]{1,0:T(8,128)(2,1)} %attend_remote.3.refs_0_) | copy-start | bytes 393220
  42.6 5.5 %collective-permute-start.13 = (bf16[256,256]{1,0:T(8,128)(2,1)}, bf16[256,256]{1,0:T(8,128)(2,1)S(1)}, u32[]{:S(2)}, u32[]{:S(2)}) collective-permute-start(bf16[256,256]{1,0:T(8,128)(2,1)} %attend_remote.3.refs_0_), channel_id=1, source_target_pairs={{0,2},{1,3},{2,0},{3,1},{4,6},{5,7},{6,4},{7,5},{8,10},{9,11},{10,... | collective-permute-start | bytes 393224 | tf_op jit(solution)/shard_map/ppermute | solution.py:36
  47.4 5.2 %collective-permute-start.10 = (bf16[256,256]{1,0:T(8,128)(2,1)}, bf16[256,256]{1,0:T(8,128)(2,1)S(1)}, u32[]{:S(2)}, u32[]{:S(2)}) collective-permute-start(bf16[256,256]{1,0:T(8,128)(2,1)} %attend_remote.2.refs_0_), channel_id=1, source_target_pairs={{0,2},{1,3},{2,0},{3,1},{4,6},{5,7},{6,4},{7,5},{8,10},{9,11},{10,... | collective-permute-start | bytes 393224 | tf_op jit(solution)/shard_map/ppermute | solution.py:36
  48.0 4.7 %collective-permute-start.12 = (bf16[256,256]{1,0:T(8,128)(2,1)S(1)}, bf16[256,256]{1,0:T(8,128)(2,1)S(1)}, u32[]{:S(2)}, u32[]{:S(2)}) collective-permute-start(bf16[256,256]{1,0:T(8,128)(2,1)S(1)} %copy-done.3), channel_id=1, source_target_pairs={{0,1},{1,0},{2,3},{3,2},{4,5},{5,4},{6,7},{7,6},{8,9},{9,8},{10,11... | collective-permute-start | bytes 393224 | tf_op jit(solution)/shard_map/ppermute | solution.py:36
  48.1 4.6 %copy-start.7 = (bf16[256,256]{1,0:T(8,128)(2,1)}, bf16[256,256]{1,0:T(8,128)(2,1)S(1)}, u32[]{:S(2)}) copy-start(bf16[256,256]{1,0:T(8,128)(2,1)S(1)} %collective-permute-done.13.refs_2_) | copy-start | bytes 393220
  48.1 4.6 %collective-permute-start.14 = (bf16[256,256]{1,0:T(8,128)(2,1)S(1)}, bf16[256,256]{1,0:T(8,128)(2,1)S(1)}, u32[]{:S(2)}, u32[]{:S(2)}) collective-permute-start(bf16[256,256]{1,0:T(8,128)(2,1)S(1)} %collective-permute-done.13.refs_2_), channel_id=1, source_target_pairs={{0,1},{1,0},{2,3},{3,2},{4,5},{5,4},{6,7},{7,6},{8,9},{9,8},{10,11... | collective-permute-start | bytes 393224 | tf_op jit(solution)/shard_map/ppermute | solution.py:36
  48.5 8.2 %collective-permute-start.9 = (bf16[256,256]{1,0:T(8,128)(2,1)}, bf16[256,256]{1,0:T(8,128)(2,1)S(1)}, u32[]{:S(2)}, u32[]{:S(2)}) collective-permute-start(bf16[256,256]{1,0:T(8,128)(2,1)} %attend_remote.2.refs_0_), channel_id=1, source_target_pairs={{0,1},{1,0},{2,3},{3,2},{4,5},{5,4},{6,7},{7,6},{8,9},{9,8},{10,11... | collective-permute-start | bytes 393224 | tf_op jit(solution)/shard_map/ppermute | solution.py:36
  52.7 4.0 %copy-start.8 = (bf16[256,256]{1,0:T(8,128)(2,1)}, bf16[256,256]{1,0:T(8,128)(2,1)S(1)}, u32[]{:S(2)}) copy-start(bf16[256,256]{1,0:T(8,128)(2,1)S(1)} %collective-permute-done.10.refs_2_) | copy-start | bytes 393220
  52.7 4.0 %collective-permute-start.11 = (bf16[256,256]{1,0:T(8,128)(2,1)S(1)}, bf16[256,256]{1,0:T(8,128)(2,1)S(1)}, u32[]{:S(2)}, u32[]{:S(2)}) collective-permute-start(bf16[256,256]{1,0:T(8,128)(2,1)S(1)} %collective-permute-done.10.refs_2_), channel_id=1, source_target_pairs={{0,1},{1,0},{2,3},{3,2},{4,5},{5,4},{6,7},{7,6},{8,9},{9,8},{10,11... | collective-permute-start | bytes 393224 | tf_op jit(solution)/shard_map/ppermute | solution.py:36
  52.7 0.7 %copy-start.10 = (bf16[256,256]{1,0:T(8,128)(2,1)}, bf16[256,256]{1,0:T(8,128)(2,1)S(1)}, u32[]{:S(2)}) copy-start(bf16[256,256]{1,0:T(8,128)(2,1)S(1)} %collective-permute-done.12.refs_1_) | copy-start | bytes 393220
  53.4 0.7 %copy-start.12 = (bf16[256,256]{1,0:T(8,128)(2,1)}, bf16[256,256]{1,0:T(8,128)(2,1)S(1)}, u32[]{:S(2)}) copy-start(bf16[256,256]{1,0:T(8,128)(2,1)S(1)} %collective-permute-done.14.refs_3_) | copy-start | bytes 393220
  56.7 0.6 %copy-start.9 = (bf16[256,256]{1,0:T(8,128)(2,1)}, bf16[256,256]{1,0:T(8,128)(2,1)S(1)}, u32[]{:S(2)}) copy-start(bf16[256,256]{1,0:T(8,128)(2,1)S(1)} %collective-permute-done.9.refs_1_) | copy-start | bytes 393220
  57.3 0.7 %copy-start.11 = (bf16[256,256]{1,0:T(8,128)(2,1)}, bf16[256,256]{1,0:T(8,128)(2,1)S(1)}, u32[]{:S(2)}) copy-start(bf16[256,256]{1,0:T(8,128)(2,1)S(1)} %collective-permute-done.11.refs_3_) | copy-start | bytes 393220

commit v2 on v1

--- a/solution.py
+++ b/solution.py
@@ -25,6 +25,9 @@
 
 def vspec():
     return pl.BlockSpec(memory_space=VMEM)
+
+
+PARAMS = pltpu.CompilerParams(vmem_limit_bytes=16 << 20)
 
 
 def sspec():
@@ -81,6 +84,7 @@
         out_shape=outs,
         in_specs=[sspec(), vspec()],
         out_specs=[vspec()] * len(outs),
+        compiler_params=PARAMS,
         name="requests",
     )(info, select)
 
@@ -134,6 +138,7 @@
         cost_estimate=pl.CostEstimate(
             flops=2 * rows * wq.shape[0] * 4 * HD, transcendentals=0, bytes_accessed=6 << 20
         ),
+        compiler_params=PARAMS,
         name="project",
     )(info, *pieces, gain, wq, wk, wv, cos, sin)
 
@@ -159,6 +164,7 @@
         out_shape=outs,
         in_specs=[sspec()] * (count + 1) + [vspec()] * 2,
         out_specs=[vspec()] * count,
+        compiler_params=PARAMS,
         name="pick_blocks",
     )(info, *asked, keys, values)
 
@@ -216,6 +222,7 @@
         cost_estimate=pl.CostEstimate(
             flops=4 * rows * rows * width, transcendentals=rows * rows * heads, bytes_accessed=2 << 20
         ),
+        compiler_params=PARAMS,
         name="attend_local",
     )(queries, keys, values)
 
@@ -264,6 +271,7 @@
         out_shape=jax.ShapeDtypeStruct((blocks * query_rows, heads * HD), bf16),
         in_specs=[vspec()] * (5 + count),
         out_specs=vspec(),
+        compiler_params=PARAMS,
         name="attend_remote",
     )(queries, m, l, o, bias, *received)
 
@@ -301,6 +309,7 @@
         cost_estimate=pl.CostEstimate(
             flops=2 * rows * w_out.shape[0] * w_out.shape[1], transcendentals=0, bytes_accessed=2 << 20
         ),
+        compiler_params=PARAMS,
         name="project_out",
     )(*args)
 

time: 61 us -> 45.5 us (0.75)
  Pallas kernels: 23.2 us -> 10.8 us
  local copies, waits for them, and re-layouts: 5.41 us -> 2.08 us
  waiting for transfers between devices: 10.2 us -> 11.7 us
  other arithmetic: 2.62 us -> 1.29 us
    pallas_call x2, Pallas kernels: 6.65 us -> 2.33 us  [attend_remote(): pl.pallas_call(functools.partial(remote_kernel, query_rows=query_rows, he...]
    unnamed x34 -> x14, local copies, waits for them, and re-layouts: 4.75 us -> 2.07 us
    pallas_call x1, Pallas kernels: 4.86 us -> 2.24 us  [project(): pl.pallas_call(functools.partial(project_kernel, pieces=count, heads=wq.s...]
    pallas_call x1, Pallas kernels: 3.17 us -> 1.22 us  [attend_local(): pl.pallas_call(functools.partial(local_kernel, query_rows=query_rows, hea...]
    pallas_call x2, Pallas kernels: 5.29 us -> 3.37 us  [project_out(): pl.pallas_call(functools.partial(output_kernel, pieces=count), grid=(1,),...]
    ppermute x9, waiting for transfers between devices: 10.1 us -> 11.4 us  [swap(): return lax.ppermute(array, axis, [(i, i ^ mask) for i in range(size)])]
    pallas_call x1, Pallas kernels: 1.65 us -> 0.77 us  [pick_blocks(): pl.pallas_call(functools.partial(send_kernel, count=count, blocks_dev=blo...]
    concatenate x1, other arithmetic: 1.03 us -> 0.21 us  [per_device(): cos = jnp.concatenate([cos, cos], axis=1)]
  transfers between devices with their start and end apart: 15 -> 15, of which waited for: 3 -> 5; matrix products, arithmetic and copies ran while one was open for 5% -> 3% of each run, Pallas kernels for 26% -> 16%
where the time goes in v2:
time: 45.5 us; the launch traced here: 45.1 us
  starting transfers between devices  19 us (42%)
  waiting for transfers between devices  11.7 us (26%)
  Pallas kernels  10.8 us (24%)
  local copies, waits for them, and re-layouts  2.08 us (5%)
  other arithmetic  1.29 us (3%)
    ppermute x9, waiting for transfers between devices, swap(): return lax.ppermute(array, axis, [(i, i ^ mask) for i in range(size)])  11.4 us
    ppermute x3, starting transfers between devices, shift_up(): lax.ppermute(array, axis, [(i, i + shift) for i in range(size - shift)])  9.52 us
    ppermute x9, starting transfers between devices, swap(): return lax.ppermute(array, axis, [(i, i ^ mask) for i in range(size)])  5.64 us
    ppermute x3, starting transfers between devices, shift_down(): lax.ppermute(array, axis, [(i, i - shift) for i in range(shift, size)])  3.88 us
    pallas_call x2, Pallas kernels, project_out(): pl.pallas_call(functools.partial(output_kernel, pieces=count), grid=(1,),...  3.37 us
    pallas_call x2, Pallas kernels, attend_remote(): pl.pallas_call(functools.partial(remote_kernel, query_rows=query_rows, he...  2.33 us
    pallas_call x1, Pallas kernels, project(): pl.pallas_call(functools.partial(project_kernel, pieces=count, heads=wq.s...  2.24 us
    unnamed x14, local copies, waits for them, and re-layouts  2.07 us
  transfers between devices with their start and end apart: 15, of which 5 were waited for; matrix products, arithmetic and copies ran while one was open for 3% of the time, Pallas kernels for 16%

profile of v2, /device:TPU:0, one launch (start us, length us, event | category | flops | bytes accessed | tf_op | source)
XLA Modules:
  0.0 45.1 jit_solution(4761830010981285083)
XLA Ops:
  0.0 3.0 %collective-permute-start.1 = (bf16[512,512]{1,0:T(8,128)(2,1)}, bf16[512,512]{1,0:T(8,128)(2,1)S(1)}, u32[]{:S(2)}, u32[]{:S(2)}) collective-permute-start(bf16[512,512]{1,0:T(8,128)(2,1)} %refs_0_.1), channel_id=1, source_target_pairs={{0,2},{1,3},{2,0},{3,1},{4,6},{5,7},{6,4},{7,5},{8,10},{9,11},{10,... | collective-permute-start | bytes 1572872 | tf_op jit(solution)/shard_map/ppermute | solution.py:39
  3.0 0.0 collective-permute-start
  3.0 0.1 pad_add_fusion.info_ref
  3.0 0.6 %copy-done.5 = s32[4,32]{1,0:T(4,128)S(1)} copy-done((s32[4,32]{1,0:T(4,128)S(1)}, s32[4,32]{1,0:T(4,128)}, u32[]{:S(2)}) %copy-start.5) | copy-done | bytes 536
  3.7 0.8 %requests.1 = (s32[8,128]{1,0:T(8,128)S(1)}, s32[8,128]{1,0:T(8,128)S(1)}, s32[8,128]{1,0:T(8,128)S(1)}, f32[3,4,64]{2,1,0:T(4,128)S(1)}) custom-call(s32[2]{0:T(128)S(1)} %pad_add_fusion.info_ref, s32[4,32]{1,0:T(4,128)S(1)} %copy-done.5), custom_call_target="tpu_custom_call" | custom-call | tf_op jit(solution)/shard_map/requests/pallas_call | solution.py:82
  4.5 1.3 %collective-permute-start.3 = (s32[8,128]{1,0:T(8,128)S(1)}, s32[8,128]{1,0:T(8,128)S(1)}, u32[]{:S(2)}, u32[]{:S(2)}) collective-permute-start(s32[8,128]{1,0:T(8,128)S(1)} %get-tuple-element.25), channel_id=1, source_target_pairs={{4,0},{8,4},{12,8},{5,1},{9,5},{13,9},{6,2},{10,6},{14,10},{7,3},{... | collective-permute-start | bytes 12296 | tf_op jit(solution)/shard_map/ppermute | solution.py:324
  5.8 1.3 %collective-permute-start.4 = (s32[8,128]{1,0:T(8,128)S(1)}, s32[8,128]{1,0:T(8,128)S(1)}, u32[]{:S(2)}, u32[]{:S(2)}) collective-permute-start(s32[8,128]{1,0:T(8,128)S(1)} %get-tuple-element.26), channel_id=1, source_target_pairs={{8,0},{12,4},{9,1},{13,5},{10,2},{14,6},{11,3},{15,7},{24,16},{28,... | collective-permute-start | bytes 12296 | tf_op jit(solution)/shard_map/ppermute | solution.py:324
  7.1 1.3 %collective-permute-start.5 = (s32[8,128]{1,0:T(8,128)S(1)}, s32[8,128]{1,0:T(8,128)S(1)}, u32[]{:S(2)}, u32[]{:S(2)}) collective-permute-start(s32[8,128]{1,0:T(8,128)S(1)} %get-tuple-element.27), channel_id=1, source_target_pairs={{12,0},{13,1},{14,2},{15,3},{28,16},{29,17},{30,18},{31,19}} | collective-permute-start | bytes 12296 | tf_op jit(solution)/shard_map/ppermute | solution.py:324
  8.4 6.7 %collective-permute-done.1.refs_2_ = bf16[512,512]{1,0:T(8,128)(2,1)S(1)} collective-permute-done((bf16[512,512]{1,0:T(8,128)(2,1)}, bf16[512,512]{1,0:T(8,128)(2,1)S(1)}, u32[]{:S(2)}, u32[]{:S(2)}) %collective-permute-start.1) | collective-permute-done | bytes 524320 | tf_op jit(solution)/shard_map/ppermute | solution.py:39
  15.1 0.0 collective-permute-start.2
  15.2 0.0 copy-start.1
  15.2 1.0 %fusion = (f32[512,64]{1,0:T(8,128)S(1)}, f32[512,64]{1,0:T(8,128)S(1)}, f32[512,64]{1,0:T(8,128)S(1)}) fusion(f32[64]{0:T(128)S(1)} %multiply_power_fusion, f32[512]{0:T(512)S(1)} %add_convert_fusion), kind=kLoop, calls=%fused_computation.4 | loop fusion | flops 65536 | bytes 395520 | tf_op jit(solution)/shard_map/neg | solution.py:348
  16.2 0.0 copy-start.2
  16.2 0.0 copy-start.3
  16.2 0.2 pad_maximum_fusion
  16.4 0.0 collective-permute-done.refs_1_
  16.4 0.6 %collective-permute-done.2.refs_3_ = bf16[512,512]{1,0:T(8,128)(2,1)S(1)} collective-permute-done((bf16[512,512]{1,0:T(8,128)(2,1)S(1)}, bf16[512,512]{1,0:T(8,128)(2,1)S(1)}, u32[]{:S(2)}, u32[]{:S(2)}) %collective-permute-start.2) | collective-permute-done | bytes 524320 | tf_op jit(solution)/shard_map/ppermute | solution.py:39
  17.0 0.2 copy-done.2
  17.3 0.2 copy-done.3
  17.4 1.0 %copy-done.4 = bf16[2048,128]{1,0:T(8,128)(2,1)S(1)} copy-done((bf16[2048,128]{1,0:T(8,128)(2,1)S(1)}, bf16[2048,128]{1,0:T(8,128)(2,1)}, u32[]{:S(2)}) %copy-start.4) | copy-done | bytes 524312
  18.5 2.2 %project.1 = (bf16[512,256]{1,0:T(8,128)(2,1)S(1)}, bf16[512,128]{1,0:T(8,128)(2,1)S(1)}, bf16[512,128]{1,0:T(8,128)(2,1)S(1)}) custom-call(s32[2]{0:T(128)S(1)} %pad_add_fusion.info_ref, bf16[512,512]{1,0:T(8,128)(2,1)S(1)} %copy-done.2, bf16[512,512]{1,0:T(8,128)(2,1)S(1)} %collective-permute-done.refs_1_, ...), custom_call_target="tpu_custom_call" | custom-call | flops 1073741824 | bytes 6291456 | tf_op jit(solution)/shard_map/project/pallas_call | solution.py:133
  20.7 0.0 collective-permute-done.3.refs_0_
  20.7 0.0 collective-permute-done.4.refs_1_
  20.7 0.0 collective-permute-done.5.refs_2_
  20.7 0.8 %pick_blocks.1 = (bf16[64,256]{1,0:T(8,128)(2,1)S(1)}, bf16[64,256]{1,0:T(8,128)(2,1)S(1)}, bf16[64,256]{1,0:T(8,128)(2,1)S(1)}) custom-call(s32[2]{0:T(128)S(1)} %pad_add_fusion.info_ref, s32[8,128]{1,0:T(8,128)S(1)} %collective-permute-done.3.refs_0_, s32[8,128]{1,0:T(8,128)S(1)} %collective-permute-done.4.refs_1_, ...), custom_call_target="tpu_custom_call" | custom-call | tf_op jit(solution)/shard_map/pick_blocks/pallas_call | solution.py:162
  21.5 3.7 %collective-permute-start.6 = (bf16[64,256]{1,0:T(8,128)(2,1)S(1)}, bf16[64,256]{1,0:T(8,128)(2,1)S(1)}, u32[]{:S(2)}, u32[]{:S(2)}) collective-permute-start(bf16[64,256]{1,0:T(8,128)(2,1)S(1)} %get-tuple-element.28), channel_id=1, source_target_pairs={{0,4},{4,8},{8,12},{1,5},{5,9},{9,13},{2,6},{6,10},{10,14},{3,7},{... | collective-permute-start | bytes 98312 | tf_op jit(solution)/shard_map/ppermute | solution.py:319
  25.3 4.5 %collective-permute-start.7 = (bf16[64,256]{1,0:T(8,128)(2,1)S(1)}, bf16[64,256]{1,0:T(8,128)(2,1)S(1)}, u32[]{:S(2)}, u32[]{:S(2)}) collective-permute-start(bf16[64,256]{1,0:T(8,128)(2,1)S(1)} %get-tuple-element.29), channel_id=1, source_target_pairs={{0,8},{4,12},{1,9},{5,13},{2,10},{6,14},{3,11},{7,15},{16,24},{20,... | collective-permute-start | bytes 98312 | tf_op jit(solution)/shard_map/ppermute | solution.py:319
  29.8 1.3 %collective-permute-start.8 = (bf16[64,256]{1,0:T(8,128)(2,1)S(1)}, bf16[64,256]{1,0:T(8,128)(2,1)S(1)}, u32[]{:S(2)}, u32[]{:S(2)}) collective-permute-start(bf16[64,256]{1,0:T(8,128)(2,1)S(1)} %get-tuple-element.30), channel_id=1, source_target_pairs={{0,12},{1,13},{2,14},{3,15},{16,28},{17,29},{18,30},{19,31}} | collective-permute-start | bytes 98312 | tf_op jit(solution)/shard_map/ppermute | solution.py:319
  31.1 1.2 %attend_local.1 = (f32[4,256,128]{2,1,0:T(8,128)S(1)}, f32[4,256,128]{2,1,0:T(8,128)S(1)}, f32[4,256,128]{2,1,0:T(8,128)S(1)}) custom-call(bf16[512,256]{1,0:T(8,128)(2,1)S(1)} %get-tuple-element.18.q_ref, bf16[512,128]{1,0:T(8,128)(2,1)S(1)} %get-tuple-element.19.k_ref.refs_3_, bf16[512,128]{1,0:T(8,128)(2,1)S(1)} %get-tuple-element.20.v_ref.refs_4_), custom_call_target="tpu_custom_call" | custom-call | flops 268435456 | bytes 2097152 | tf_op jit(solution)/shard_map/attend_local/pallas_call | solution.py:217
  32.3 0.0 collective-permute-done.6.refs_0_
  32.3 0.0 collective-permute-done.7.refs_1_
  32.3 0.3 collective-permute-done.8.refs_2_
  32.6 1.2 %attend_remote.3.refs_0_ = bf16[256,256]{1,0:T(8,128)(2,1)S(1)} custom-call(bf16[512,256]{1,0:T(8,128)(2,1)S(1)} %get-tuple-element.18.q_ref, f32[4,256,128]{2,1,0:T(8,128)S(1)} %get-tuple-element.21.m_ref, f32[4,256,128]{2,1,0:T(8,128)S(1)} %get-tuple-element.22.l_ref, f32[4,256,128]{2,1,0:T(8,128)S(1)} %get-tuple-element.23.o_ref, ...), custom_call_target="tpu_custom_call" | custom-call | tf_op jit(solution)/shard_map/attend_remote/pallas_call | solution.py:262
  33.8 0.0 copy-start
  33.8 1.6 %collective-permute-start.13 = (bf16[256,256]{1,0:T(8,128)(2,1)S(1)}, bf16[256,256]{1,0:T(8,128)(2,1)S(1)}, u32[]{:S(2)}, u32[]{:S(2)}) collective-permute-start(bf16[256,256]{1,0:T(8,128)(2,1)S(1)} %attend_remote.3.refs_0_), channel_id=1, source_target_pairs={{0,2},{1,3},{2,0},{3,1},{4,6},{5,7},{6,4},{7,5},{8,10},{9,11},{10,... | collective-permute-start | bytes 393224 | tf_op jit(solution)/shard_map/ppermute | solution.py:39
  35.4 1.2 %attend_remote.2.refs_0_ = bf16[256,256]{1,0:T(8,128)(2,1)S(1)} custom-call(bf16[512,256]{1,0:T(8,128)(2,1)S(1)} %get-tuple-element.18.q_ref, f32[4,256,128]{2,1,0:T(8,128)S(1)} %get-tuple-element.21.m_ref, f32[4,256,128]{2,1,0:T(8,128)S(1)} %get-tuple-element.22.l_ref, f32[4,256,128]{2,1,0:T(8,128)S(1)} %get-tuple-element.23.o_ref, ...), custom_call_target="tpu_custom_call" | custom-call | tf_op jit(solution)/shard_map/attend_remote/pallas_call | solution.py:262
  36.6 0.6 %collective-permute-start.10 = (bf16[256,256]{1,0:T(8,128)(2,1)S(1)}, bf16[256,256]{1,0:T(8,128)(2,1)S(1)}, u32[]{:S(2)}, u32[]{:S(2)}) collective-permute-start(bf16[256,256]{1,0:T(8,128)(2,1)S(1)} %attend_remote.2.refs_0_), channel_id=1, source_target_pairs={{0,2},{1,3},{2,0},{3,1},{4,6},{5,7},{6,4},{7,5},{8,10},{9,11},{10,... | collective-permute-start | bytes 393224 | tf_op jit(solution)/shard_map/ppermute | solution.py:39
  37.2 0.0 collective-permute-start.12
  37.2 2.1 %collective-permute-done.13.refs_2_ = bf16[256,256]{1,0:T(8,128)(2,1)S(1)} collective-permute-done((bf16[256,256]{1,0:T(8,128)(2,1)S(1)}, bf16[256,256]{1,0:T(8,128)(2,1)S(1)}, u32[]{:S(2)}, u32[]{:S(2)}) %collective-permute-start.13) | collective-permute-done | bytes 131104 | tf_op jit(solution)/shard_map/ppermute | solution.py:39
  39.3 0.0 collective-permute-start.14
  39.3 0.5 %collective-permute-start.9 = (bf16[256,256]{1,0:T(8,128)(2,1)S(1)}, bf16[256,256]{1,0:T(8,128)(2,1)S(1)}, u32[]{:S(2)}, u32[]{:S(2)}) collective-permute-start(bf16[256,256]{1,0:T(8,128)(2,1)S(1)} %attend_remote.2.refs_0_), channel_id=1, source_target_pairs={{0,1},{1,0},{2,3},{3,2},{4,5},{5,4},{6,7},{7,6},{8,9},{9,8},{10,11... | collective-permute-start | bytes 393224 | tf_op jit(solution)/shard_map/ppermute | solution.py:39
  39.8 1.9 %collective-permute-done.10.refs_2_ = bf16[256,256]{1,0:T(8,128)(2,1)S(1)} collective-permute-done((bf16[256,256]{1,0:T(8,128)(2,1)S(1)}, bf16[256,256]{1,0:T(8,128)(2,1)S(1)}, u32[]{:S(2)}, u32[]{:S(2)}) %collective-permute-start.10) | collective-permute-done | bytes 131104 | tf_op jit(solution)/shard_map/ppermute | solution.py:39
  41.7 0.0 collective-permute-start.11
  41.7 0.0 collective-permute-done.12.refs_1_
  41.7 0.0 collective-permute-done.14.refs_3_
  41.7 1.7 %project_out.2.refs_5_ = bf16[512,512]{1,0:T(8,128)(2,1)} custom-call(s32[2]{0:T(128)S(1)} %pad_add_fusion.info_ref, bf16[256,256]{1,0:T(8,128)(2,1)S(1)} %attend_remote.3.refs_0_, bf16[256,256]{1,0:T(8,128)(2,1)S(1)} %collective-permute-done.12.refs_1_, bf16[256,256]{1,0:T(8,128)(2,1)S(1)} %collective-permute-done.13.refs_2_, ...), custom_call_target="tpu_custom_call" | custom-call | flops 268435456 | bytes 2097152 | tf_op jit(solution)/shard_map/project_out/pallas_call | solution.py:302
  43.4 0.0 collective-permute-done.9.refs_1_
  43.4 1.7 %project_out.3 = bf16[512,512]{1,0:T(8,128)(2,1)} custom-call(s32[2]{0:T(128)S(1)} %pad_add_fusion.info_ref, bf16[256,256]{1,0:T(8,128)(2,1)S(1)} %attend_remote.2.refs_0_, bf16[256,256]{1,0:T(8,128)(2,1)S(1)} %collective-permute-done.9.refs_1_, bf16[256,256]{1,0:T(8,128)(2,1)S(1)} %collective-permute-done.10.refs_2_, ...), custom_call_target="tpu_custom_call", output_to_operand_aliasing={{}: (6, {})} | custom-call | flops 268435456 | bytes 2097152 | tf_op jit(solution)/shard_map/project_out/pallas_call | solution.py:302
  (10 shorter events, 0.0 us)
Async XLA Ops:
  0.0 15.1 %collective-permute-start.1 = (bf16[512,512]{1,0:T(8,128)(2,1)}, bf16[512,512]{1,0:T(8,128)(2,1)S(1)}, u32[]{:S(2)}, u32[]{:S(2)}) collective-permute-start(bf16[512,512]{1,0:T(8,128)(2,1)} %refs_0_.1), channel_id=1, source_target_pairs={{0,2},{1,3},{2,0},{3,1},{4,6},{5,7},{6,4},{7,5},{8,10},{9,11},{10,... | collective-permute-start | bytes 1572872 | tf_op jit(solution)/shard_map/ppermute | solution.py:39
  3.0 13.4 %collective-permute-start = (bf16[512,512]{1,0:T(8,128)(2,1)}, bf16[512,512]{1,0:T(8,128)(2,1)S(1)}, u32[]{:S(2)}, u32[]{:S(2)}) collective-permute-start(bf16[512,512]{1,0:T(8,128)(2,1)} %refs_0_.1), channel_id=1, source_target_pairs={{0,1},{1,0},{2,3},{3,2},{4,5},{5,4},{6,7},{7,6},{8,9},{9,8},{10,11... | collective-permute-start | bytes 1572872 | tf_op jit(solution)/shard_map/ppermute | solution.py:39
  3.0 0.7 %copy-start.5 = (s32[4,32]{1,0:T(4,128)S(1)}, s32[4,32]{1,0:T(4,128)}, u32[]{:S(2)}) copy-start(s32[4,32]{1,0:T(4,128)} %select_ref.1) | copy-start | bytes 1540
  4.5 10.6 %copy-start.6 = (bf16[2048]{0:T(1024)(128)(2,1)S(1)}, bf16[2048]{0:T(1024)(128)(2,1)}, u32[]{:S(2)}) copy-start(bf16[2048]{0:T(1024)(128)(2,1)} %param.8) | copy-start | bytes 12292
  4.5 16.2 %collective-permute-start.3 = (s32[8,128]{1,0:T(8,128)S(1)}, s32[8,128]{1,0:T(8,128)S(1)}, u32[]{:S(2)}, u32[]{:S(2)}) collective-permute-start(s32[8,128]{1,0:T(8,128)S(1)} %get-tuple-element.25), channel_id=1, source_target_pairs={{4,0},{8,4},{12,8},{5,1},{9,5},{13,9},{6,2},{10,6},{14,10},{7,3},{... | collective-permute-start | bytes 12296 | tf_op jit(solution)/shard_map/ppermute | solution.py:324
  5.8 14.9 %collective-permute-start.4 = (s32[8,128]{1,0:T(8,128)S(1)}, s32[8,128]{1,0:T(8,128)S(1)}, u32[]{:S(2)}, u32[]{:S(2)}) collective-permute-start(s32[8,128]{1,0:T(8,128)S(1)} %get-tuple-element.26), channel_id=1, source_target_pairs={{8,0},{12,4},{9,1},{13,5},{10,2},{14,6},{11,3},{15,7},{24,16},{28,... | collective-permute-start | bytes 12296 | tf_op jit(solution)/shard_map/ppermute | solution.py:324
  7.1 13.6 %collective-permute-start.5 = (s32[8,128]{1,0:T(8,128)S(1)}, s32[8,128]{1,0:T(8,128)S(1)}, u32[]{:S(2)}, u32[]{:S(2)}) collective-permute-start(s32[8,128]{1,0:T(8,128)S(1)} %get-tuple-element.27), channel_id=1, source_target_pairs={{12,0},{13,1},{14,2},{15,3},{28,16},{29,17},{30,18},{31,19}} | collective-permute-start | bytes 12296 | tf_op jit(solution)/shard_map/ppermute | solution.py:324
  15.1 1.9 %collective-permute-start.2 = (bf16[512,512]{1,0:T(8,128)(2,1)S(1)}, bf16[512,512]{1,0:T(8,128)(2,1)S(1)}, u32[]{:S(2)}, u32[]{:S(2)}) collective-permute-start(bf16[512,512]{1,0:T(8,128)(2,1)S(1)} %collective-permute-done.1.refs_2_), channel_id=1, source_target_pairs={{0,1},{1,0},{2,3},{3,2},{4,5},{5,4},{6,7},{7,6},{8,9},{9,8},{10,11... | collective-permute-start | bytes 1572872 | tf_op jit(solution)/shard_map/ppermute | solution.py:39
  15.2 1.9 %copy-start.1 = (bf16[2048,256]{1,0:T(8,128)(2,1)S(1)}, bf16[2048,256]{1,0:T(8,128)(2,1)}, u32[]{:S(2)}) copy-start(bf16[2048,256]{1,0:T(8,128)(2,1)} %refs_5_.1) | copy-start | bytes 3145732
  16.2 1.1 %copy-start.2 = (bf16[512,512]{1,0:T(8,128)(2,1)S(1)}, bf16[512,512]{1,0:T(8,128)(2,1)}, u32[]{:S(2)}) copy-start(bf16[512,512]{1,0:T(8,128)(2,1)} %refs_0_.1) | copy-start | bytes 1572868
  16.2 1.2 %copy-start.3 = (bf16[2048,128]{1,0:T(8,128)(2,1)S(1)}, bf16[2048,128]{1,0:T(8,128)(2,1)}, u32[]{:S(2)}) copy-start(bf16[2048,128]{1,0:T(8,128)(2,1)} %refs_6_.1) | copy-start | bytes 1572868
  17.4 1.0 %copy-start.4 = (bf16[2048,128]{1,0:T(8,128)(2,1)S(1)}, bf16[2048,128]{1,0:T(8,128)(2,1)}, u32[]{:S(2)}) copy-start(bf16[2048,128]{1,0:T(8,128)(2,1)} %refs_7_.1) | copy-start | bytes 1572868
  21.5 10.8 %collective-permute-start.6 = (bf16[64,256]{1,0:T(8,128)(2,1)S(1)}, bf16[64,256]{1,0:T(8,128)(2,1)S(1)}, u32[]{:S(2)}, u32[]{:S(2)}) collective-permute-start(bf16[64,256]{1,0:T(8,128)(2,1)S(1)} %get-tuple-element.28), channel_id=1, source_target_pairs={{0,4},{4,8},{8,12},{1,5},{5,9},{9,13},{2,6},{6,10},{10,14},{3,7},{... | collective-permute-start | bytes 98312 | tf_op jit(solution)/shard_map/ppermute | solution.py:319
  25.3 7.0 %collective-permute-start.7 = (bf16[64,256]{1,0:T(8,128)(2,1)S(1)}, bf16[64,256]{1,0:T(8,128)(2,1)S(1)}, u32[]{:S(2)}, u32[]{:S(2)}) collective-permute-start(bf16[64,256]{1,0:T(8,128)(2,1)S(1)} %get-tuple-element.29), channel_id=1, source_target_pairs={{0,8},{4,12},{1,9},{5,13},{2,10},{6,14},{3,11},{7,15},{16,24},{20,... | collective-permute-start | bytes 98312 | tf_op jit(solution)/shard_map/ppermute | solution.py:319
  29.8 2.9 %collective-permute-start.8 = (bf16[64,256]{1,0:T(8,128)(2,1)S(1)}, bf16[64,256]{1,0:T(8,128)(2,1)S(1)}, u32[]{:S(2)}, u32[]{:S(2)}) collective-permute-start(bf16[64,256]{1,0:T(8,128)(2,1)S(1)} %get-tuple-element.30), channel_id=1, source_target_pairs={{0,12},{1,13},{2,14},{3,15},{16,28},{17,29},{18,30},{19,31}} | collective-permute-start | bytes 98312 | tf_op jit(solution)/shard_map/ppermute | solution.py:319
  33.8 7.9 %copy-start = (bf16[1024,512]{1,0:T(8,128)(2,1)S(1)}, bf16[1024,512]{1,0:T(8,128)(2,1)}, u32[]{:S(2)}) copy-start(bf16[1024,512]{1,0:T(8,128)(2,1)} %refs_4_.3) | copy-start | bytes 3145732
  33.8 5.4 %collective-permute-start.13 = (bf16[256,256]{1,0:T(8,128)(2,1)S(1)}, bf16[256,256]{1,0:T(8,128)(2,1)S(1)}, u32[]{:S(2)}, u32[]{:S(2)}) collective-permute-start(bf16[256,256]{1,0:T(8,128)(2,1)S(1)} %attend_remote.3.refs_0_), channel_id=1, source_target_pairs={{0,2},{1,3},{2,0},{3,1},{4,6},{5,7},{6,4},{7,5},{8,10},{9,11},{10,... | collective-permute-start | bytes 393224 | tf_op jit(solution)/shard_map/ppermute | solution.py:39
  36.6 5.2 %collective-permute-start.10 = (bf16[256,256]{1,0:T(8,128)(2,1)S(1)}, bf16[256,256]{1,0:T(8,128)(2,1)S(1)}, u32[]{:S(2)}, u32[]{:S(2)}) collective-permute-start(bf16[256,256]{1,0:T(8,128)(2,1)S(1)} %attend_remote.2.refs_0_), channel_id=1, source_target_pairs={{0,2},{1,3},{2,0},{3,1},{4,6},{5,7},{6,4},{7,5},{8,10},{9,11},{10,... | collective-permute-start | bytes 393224 | tf_op jit(solution)/shard_map/ppermute | solution.py:39
  37.2 4.6 %collective-permute-start.12 = (bf16[256,256]{1,0:T(8,128)(2,1)S(1)}, bf16[256,256]{1,0:T(8,128)(2,1)S(1)}, u32[]{:S(2)}, u32[]{:S(2)}) collective-permute-start(bf16[256,256]{1,0:T(8,128)(2,1)S(1)} %attend_remote.3.refs_0_), channel_id=1, source_target_pairs={{0,1},{1,0},{2,3},{3,2},{4,5},{5,4},{6,7},{7,6},{8,9},{9,8},{10,11... | collective-permute-start | bytes 393224 | tf_op jit(solution)/shard_map/ppermute | solution.py:39
  39.3 2.5 %collective-permute-start.14 = (bf16[256,256]{1,0:T(8,128)(2,1)S(1)}, bf16[256,256]{1,0:T(8,128)(2,1)S(1)}, u32[]{:S(2)}, u32[]{:S(2)}) collective-permute-start(bf16[256,256]{1,0:T(8,128)(2,1)S(1)} %collective-permute-done.13.refs_2_), channel_id=1, source_target_pairs={{0,1},{1,0},{2,3},{3,2},{4,5},{5,4},{6,7},{7,6},{8,9},{9,8},{10,11... | collective-permute-start | bytes 393224 | tf_op jit(solution)/shard_map/ppermute | solution.py:39
  39.3 4.2 %collective-permute-start.9 = (bf16[256,256]{1,0:T(8,128)(2,1)S(1)}, bf16[256,256]{1,0:T(8,128)(2,1)S(1)}, u32[]{:S(2)}, u32[]{:S(2)}) collective-permute-start(bf16[256,256]{1,0:T(8,128)(2,1)S(1)} %attend_remote.2.refs_0_), channel_id=1, source_target_pairs={{0,1},{1,0},{2,3},{3,2},{4,5},{5,4},{6,7},{7,6},{8,9},{9,8},{10,11... | collective-permute-start | bytes 393224 | tf_op jit(solution)/shard_map/ppermute | solution.py:39
  41.7 1.7 %collective-permute-start.11 = (bf16[256,256]{1,0:T(8,128)(2,1)S(1)}, bf16[256,256]{1,0:T(8,128)(2,1)S(1)}, u32[]{:S(2)}, u32[]{:S(2)}) collective-permute-start(bf16[256,256]{1,0:T(8,128)(2,1)S(1)} %collective-permute-done.10.refs_2_), channel_id=1, source_target_pairs={{0,1},{1,0},{2,3},{3,2},{4,5},{5,4},{6,7},{7,6},{8,9},{9,8},{10,11... | collective-permute-start | bytes 393224 | tf_op jit(solution)/shard_map/ppermute | solution.py:39
